TPU v7x, 256 devices: a whole 4x4x8 slice. The times are simulated.
256 devices in a mesh: sp: 64 (over z, x, core), tp: 4 (over y).
Axes of the slice: x: 4, y: 4, z: 8, core: 2. Of those that a mesh axis runs over, the one named last changes fastest.
Arguments:
- signal: bfloat16 [8192, 1024], P('sp', 'tp'), may hold values from -6 to 6
- step_log: float32 [8192, 64], P('sp', 'tp'), may hold values from -9 to -1.9
- forget_log: float32 [8192, 64], P('sp', 'tp'), may hold values from -1.4 to 0
- damping: float32 [64, 64], P('tp'), may hold values from 0.001 to 1.6
- freq: float32 [64, 64], P('tp'), may hold values from 0 to 50.26544
- in_re: bfloat16 [64, 64, 16], P('tp'), may hold values from -1 to 1
- in_im: bfloat16 [64, 64, 16], P('tp'), may hold values from -1 to 1
- out_re: bfloat16 [64, 16, 64], P('tp'), may hold values from -4 to 4
- out_im: bfloat16 [64, 16, 64], P('tp'), may hold values from -4 to 4
- skip: float32 [1024], P('tp'), may hold values from -4 to 4
- w_out: bfloat16 [1024, 2048], P('tp'), may hold values from -0.1875 to 0.1875
- residual: bfloat16 [8192, 2048], P('sp', 'tp'), may hold values from -60 to 60
- norm_gain: bfloat16 [2048], P('tp'), may hold values from 0.099609375 to 1.8984375
- w_gate: bfloat16 [2048, 5632], P('sp', 'tp'), may hold values from -0.125 to 0.125
- w_up: bfloat16 [2048, 5632], P('sp', 'tp'), may hold values from -0.125 to 0.125
- w_down: bfloat16 [5632, 2048], P('tp', 'sp'), may hold values from -0.078125 to 0.078125
Outputs:
- output: bfloat16 [8192, 2048], P('sp', 'tp')
All inputs are finite; a program needn't handle non-finite values.
Results may differ from a plain program's by a relative error of at most 0.012.
Values may be sent and summed in bfloat16 or wider, within the bound.
No kernel may reach another device: no remote copies, remote signals or barrier semaphores. Data moves between devices by JAX's collectives and lax.ppermute only.
A program may use at most 64 MiB of HBM per device.

v0:
```python
import jax
import jax.numpy as jnp
from jax import lax
from jax.sharding import Mesh
from jax.sharding import PartitionSpec as P

SP = ("sp_0", "sp_1", "sp_2")


EPS = 1e-06


def sent_together(arrays, axis, dim, along):
    both = jnp.concatenate(arrays, axis=along)
    filled, at, done = (lax.all_gather(both, axis, axis=dim, tiled=True), 0, [])
    for a in arrays:
        done.append(lax.slice_in_dim(filled, at, at + a.shape[along], axis=along))
        at += a.shape[along]
    return tuple(done)


def filled_with(x, identity):
    return jax.tree.map(
        lambda part, zero: jnp.zeros_like(part) + jnp.asarray(zero, part.dtype), x, identity
    )


def gathered_once(x, axis):
    leaves = jax.tree.leaves(x)
    turns = sorted(range(len(leaves)), key=lambda k: -leaves[k].size)
    width = (1, *leaves[turns[0]].shape)[-1]
    lines = [
        jnp.pad(leaves[k].reshape(-1), (0, -leaves[k].size % width)).reshape(-1, width)
        for k in turns
    ]
    both, at, found = (lax.all_gather(jnp.concatenate(lines), axis), 0, {})
    for k, line in zip(turns, lines):
        section = both[:, at : at + len(line)].reshape(len(both), -1)
        found[k] = section[:, : leaves[k].size].reshape(-1, *leaves[k].shape)
        at += len(line)
    numbers = iter(range(len(leaves)))
    return jax.tree.map(lambda _: found[next(numbers)], x)


def prefix_by_axis(x, axes, combine, identity):
    before = start = filled_with(x, identity)
    subtotal = x
    for axis in reversed(axes):
        count, position = (lax.axis_size(axis), lax.axis_index(axis))
        pieces = gathered_once(subtotal, axis)
        inside, subtotal = (start, start)
        for k in range(count):
            passed = k < position
            subtotal = combine(subtotal, jax.tree.map(lambda part: part[k], pieces))
            inside = jax.tree.map(lambda new, old: jnp.where(passed, new, old), subtotal, inside)
        before = combine(inside, before)
    return before


def cut_along(x, dim, count):
    before, after = (x.shape[:dim], x.shape[dim + 1 :])
    return jnp.moveaxis(x.reshape(*before, count, -1, *after), dim, 0)


def sent_and_summed(x, axis, dim):
    count = lax.axis_size(axis)
    pieces = lax.all_to_all(cut_along(x, dim, count), axis, 0, 0, tiled=True)
    return jnp.sum(pieces.astype(jnp.float32), axis=0)


def copy_for_each(x, axis):
    count = lax.axis_size(axis)
    return lax.all_to_all(jnp.broadcast_to(x[None], (count, *x.shape)), axis, 0, 0, tiled=True)


def of_everyone(x, axis):
    everything = copy_for_each(x, axis)
    return jnp.sum(everything, axis=0)


def laid_out(pieces, dim):
    pieces = jnp.moveaxis(pieces, 0, dim)
    shape = pieces.shape
    return pieces.reshape(*shape[:dim], shape[dim] * shape[dim + 1], *shape[dim + 2 :])


def gathered_copies(x, axis, dim):
    return laid_out(copy_for_each(x, axis), dim)


def combine(earlier, later):
    first_are, first_aim, first_bre, first_bim = earlier
    second_are, second_aim, second_bre, second_bim = later
    return (
        second_are * first_are - second_aim * first_aim,
        second_are * first_aim + second_aim * first_are,
        second_are * first_bre - second_aim * first_bim + second_bre,
        second_are * first_bim + second_aim * first_bre + second_bim,
    )


def collect(w_gate, w_up, w_down):
    gate_values_wide, up_full = sent_together((w_gate, w_up), SP, 0, 1)
    down_full = lax.all_gather(w_down, SP, axis=1, tiled=True)
    return (gate_values_wide, up_full, down_full)


def local_states(elements, length, flat):
    span = 8
    blocks = tuple((item.reshape(length // span, span, flat) for item in elements))

    def advance(carry, block):
        collected = []
        for offset in range(span):
            carry = combine(carry, tuple((member[offset] for member in block)))
            collected.append(carry)
        stacked = tuple((jnp.stack([entry[number] for entry in collected]) for number in range(4)))
        return (carry, stacked)

    unity = jnp.ones((flat,), jnp.float32)
    nothing = jnp.zeros((flat,), jnp.float32)
    finals, stacked = lax.scan(advance, (unity, nothing, nothing, nothing), blocks)
    return (finals, tuple((member.reshape(length, flat) for member in stacked)))


def state_mixer(signal, step_log, forget_log, damping, freq, in_re, in_im, out_re, out_im, skip):
    length = signal.shape[0]
    groups, states = damping.shape
    width = in_re.shape[2]
    step = jnp.exp(step_log)[:, :, None]
    magnitude = jnp.exp(-damping[None] * step)
    angle = freq[None] * step
    decay_re = magnitude * jnp.cos(angle)
    decay_im = magnitude * jnp.sin(angle)
    denom = damping * damping + freq * freq
    factor_re = (-(decay_re - 1.0) * damping + decay_im * freq) / denom
    factor_im = (-decay_im * damping - (decay_re - 1.0) * freq) / denom
    keep = jnp.exp(forget_log)[:, :, None]
    rows = signal.reshape(length, groups, width)
    both_in = jnp.concatenate([in_re, in_im], axis=1)
    driven = jnp.einsum("tgc,gpc->tgp", rows, both_in, preferred_element_type=jnp.float32)
    source_re = driven[:, :, :states]
    source_im = driven[:, :, states:]
    drive_re = factor_re * source_re - factor_im * source_im
    drive_im = factor_re * source_im + factor_im * source_re
    flat = groups * states
    elements = (
        (keep * decay_re).reshape(length, flat),
        (keep * decay_im).reshape(length, flat),
        drive_re.reshape(length, flat),
        drive_im.reshape(length, flat),
    )
    finals, (running_real, cum_im, local_re, local_im) = local_states(elements, length, flat)
    unity = jnp.ones((flat,), jnp.float32)
    nothing = jnp.zeros((flat,), jnp.float32)
    prior = prefix_by_axis(finals, SP, combine, (unity, nothing, nothing, nothing))
    state_re = local_re + running_real * prior[2][None] - cum_im * prior[3][None]
    state_im = local_im + running_real * prior[3][None] + cum_im * prior[2][None]
    state_readout = jnp.einsum(
        "myq,yzq->myz", state_re.reshape(length, groups, states), out_re.astype(jnp.float32)
    ) - jnp.einsum(
        "myq,yzq->myz", state_im.reshape(length, groups, states), out_im.astype(jnp.float32)
    )
    value = state_readout.reshape(length, groups * width) + skip * signal.astype(jnp.float32)
    return jax.nn.gelu(value).astype(jnp.bfloat16)


def local(
    signal,
    step_log,
    forget_log,
    damping,
    freq,
    in_re,
    in_im,
    out_re,
    out_im,
    skip,
    w_out,
    residual,
    norm_gain,
    w_gate,
    w_up,
    w_down,
):
    mixed = state_mixer(
        signal, step_log, forget_log, damping, freq, in_re, in_im, out_re, out_im, skip
    )
    partial_value = jnp.dot(mixed, w_out, preferred_element_type=jnp.float32)
    gate_values_wide, up_full, down_full = collect(w_gate, w_up, w_down)
    model_width = w_out.shape[1]
    projected = sent_and_summed(partial_value.astype(jnp.bfloat16), "tp", 1)
    middle = (residual.astype(jnp.float32) + projected).astype(jnp.bfloat16)
    middle_wide = middle.astype(jnp.float32)
    squares = of_everyone(jnp.sum(middle_wide * middle_wide, axis=1), "tp")
    normed = (
        middle_wide
        * lax.rsqrt(squares[:, None] / model_width + EPS)
        * norm_gain.astype(jnp.float32)
    ).astype(jnp.bfloat16)
    piece = gathered_copies(normed, "tp", 1)
    gate = jnp.dot(piece, gate_values_wide, preferred_element_type=jnp.float32)
    up_projected = jnp.dot(piece, up_full, preferred_element_type=jnp.float32)
    hidden = (jax.nn.silu(gate) * up_projected).astype(jnp.bfloat16)
    down_terms = jnp.dot(hidden, down_full, preferred_element_type=jnp.float32)
    down = sent_and_summed(down_terms.astype(jnp.bfloat16), "tp", 1)
    return (middle_wide + 0.5 * down).astype(jnp.bfloat16)


def solution(mesh):
    torus = Mesh(mesh.devices.reshape(8, 4, 2, mesh.shape["tp"]), ("sp_0", "sp_1", "sp_2", "tp"))
    return jax.shard_map(
        local,
        mesh=torus,
        in_specs=(
            P(SP, "tp"),
            P(SP, "tp"),
            P(SP, "tp"),
            P("tp", None),
            P("tp", None),
            P("tp", None, None),
            P("tp", None, None),
            P("tp", None, None),
            P("tp", None, None),
            P("tp"),
            P("tp", None),
            P(SP, "tp"),
            P("tp"),
            P(SP, "tp"),
            P(SP, "tp"),
            P("tp", SP),
        ),
        out_specs=P(SP, "tp"),
        check_vma=False,
    )
```

profile of v0, /device:TPU:2, one launch (start us, length us, event | category | flops | bytes accessed | tf_op | source)
XLA Modules:
  0.0 210.5 jit_solution(6707447612949672171)
XLA Ops:
  6.5 1.7 pad_maximum_fusion
  12.4 1.5 convolution_bitcast_fusion
  13.9 3.4 %multiply_add_fusion.9 = (f32[128,16,64]{0,2,1:T(8,128)S(1)}, f32[128,16,64]{0,2,1:T(8,128)S(1)}) fusion(f32[128,16,128]{0,2,1:T(8,128)S(1)} %convolution_bitcast_fusion, f32[16,64]{1,0:T(8,128)S(1)} %get-tuple-element.320, f32[16,64]{1,0:T(8,128)} %param.21, f32[16,64]{1,0:T(8,128)} %param.22, f32[128,16]{0,1:T(8,128)S(1)} %exp.18, ...), kind=kLoop, calls=%fused_computation.97 | loop fusion | flops 2752512 | bytes 2121728 | tf_op jit(solution)/shard_map/add | solution.py:145
  22.0 2.1 multiply_multiply_fusion
  24.1 64.2 %while.25 = (s32[]{:T(128)}, f32[1024]{0:T(1024)S(1)}, f32[1024]{0:T(1024)S(1)}, f32[1024]{0:T(1024)S(1)}, f32[1024]{0:T(1024)S(1)}, /*index=5*/f32[16,8,1024]{2...) while((s32[]{:T(128)}, f32[1024]{0:T(1024)S(1)}, ...), condition=%wide.region_1.2_spmd.clone, body=%wide.region_0.1_spmd.clone.sunk | while | flops 118794 | bytes 1156516 | solution.py:122
  29.4 1.3 constant_dynamic-slice_fusion.36
  56.3 1.3 constant_dynamic-slice_fusion.38
  61.5 1.2 constant_dynamic-slice_fusion.36
  81.5 1.3 constant_dynamic-slice_fusion.36
  88.3 1.8 all-gather.3
  90.3 11.9 %all-gather.4 = f32[4,4,1024]{2,1,0:T(4,128)S(1)} all-gather(f32[1,4,1024]{2,1,0:T(4,128)S(1)} %maximum_bitcast_fusion.1), channel_id=3, replica_groups=mesh['sp_0'=8,'sp_1'=4,'sp_2'=2,'tp'=4] {'sp_1'}, dimensions={0}, use_global_device_ids=true | all-gather | bytes 81920 | tf_op jit(solution)/shard_map/all_gather | solution.py:36
  102.4 28.3 %all-gather.5 = f32[8,4,1024]{2,1,0:T(4,128)S(1)} all-gather(f32[1,4,1024]{2,1,0:T(4,128)S(1)} %maximum_bitcast_fusion.2), channel_id=4, replica_groups=mesh['sp_0'=8,'sp_1'=4,'sp_2'=2,'tp'=4] {'sp_0'}, dimensions={0}, use_global_device_ids=true | all-gather | bytes 147456 | tf_op jit(solution)/shard_map/all_gather | solution.py:36
  137.6 1.3 reshape.1716
  138.9 1.3 reshape.1717
  140.3 2.3 %reshape.1722 = f32[128,16,64]{2,1,0:T(8,128)} reshape(f32[16,8,1024]{2,1,0:T(8,128)} %get-tuple-element.85) | data formatting | bytes 1048576 | tf_op jit(solution)/shard_map/reshape | solution.py:123
  142.6 2.3 %reshape.1723 = f32[128,16,64]{2,1,0:T(8,128)} reshape(f32[16,8,1024]{2,1,0:T(8,128)} %get-tuple-element.86) | data formatting | bytes 1048576 | tf_op jit(solution)/shard_map/reshape | solution.py:123
  145.9 1.9 multiply_add_fusion.8
  149.1 12.3 %all_to_all.21 = bf16[4,128,512]{2,1,0:T(8,128)(2,1)S(1)} all-to-all(bf16[4,128,512]{2,1,0:T(8,128)(2,1)S(1)} %bitcast.516), channel_id=1, replica_groups=mesh['sp_0'=8,'sp_1'=4,'sp_2'=2,'tp'=4] {'tp'}, dimensions={0} | all-to-all | bytes 1048576 | tf_op jit(solution)/shard_map/all_to_all | solution.py:67
  162.2 3.2 %all-to-all-start.1 = ((f32[4,1,128]{2,1,0:T(1,128)}), f32[4,1,128]{2,1,0:T(1,128)S(1)}, u32[]{:S(2)}, u32[]{:S(2)}) async-start(f32[4,1,128]{2,1,0:T(1,128)} %broadcast_in_dim.17), calls=%async_computation.1 | async-start | bytes 4096 | tf_op jit(solution)/shard_map/all_to_all | solution.py:73
  165.5 5.2 %all-to-all-done.1 = f32[4,1,128]{2,1,0:T(1,128)S(1)} async-done(((f32[4,1,128]{2,1,0:T(1,128)}), f32[4,1,128]{2,1,0:T(1,128)S(1)}, u32[]{:S(2)}, u32[]{:S(2)}) %all-to-all-start.1) | async-done | bytes 2080 | tf_op jit(solution)/shard_map/all_to_all | solution.py:73
  171.0 10.5 %all_to_all.22 = bf16[4,128,512]{1,2,0:T(8,128)(2,1)S(1)} all-to-all(bf16[4,128,512]{1,2,0:T(8,128)(2,1)S(1)} %broadcast_in_dim.18), channel_id=1, replica_groups=mesh['sp_0'=8,'sp_1'=4,'sp_2'=2,'tp'=4] {'tp'}, dimensions={0} | all-to-all | bytes 1048576 | tf_op jit(solution)/shard_map/all_to_all | solution.py:73
  181.5 3.6 %fusion.2 = f32[128,1408]{1,0:T(8,128)S(1)} fusion(bf16[128,2048]{0,1:T(8,128)(2,1)S(1)} %bitcast.556, bf16[2048,2816]{1,0:T(8,128)(2,1)} %all-gather.9.cloned.1.call-done), kind=kOutput, calls=%fused_computation.70 | convolution fusion | flops 738197504 | bytes 7012352 | tf_op jit(solution)/shard_map/dot_general | solution.py:202
  185.2 7.2 %convolution_convert_fusion.1 = bf16[128,2048]{1,0:T(8,128)(2,1)S(1)} fusion(bf16[1408,2048]{0,1:T(8,128)(2,1)} %all-gather.11.cloned.1.call-done, bf16[128,2048]{0,1:T(8,128)(2,1)S(1)} %bitcast.557, bf16[2048,2816]{1,0:T(8,128)(2,1)} %all-gather.9.cloned.1.call-done, f32[128,1408]{1,0:T(8,128)S(1)} %fusion.2), kind=kOutput, calls=%fused_computation.75 | convolution fusion | flops 1477738496 | bytes 13303808 | tf_op jit(solution)/shard_map/dot_general | solution.py:205
  192.4 10.5 %all_to_all.23 = bf16[4,128,512]{2,1,0:T(8,128)(2,1)S(1)} all-to-all(bf16[4,128,512]{2,1,0:T(8,128)(2,1)S(1)} %bitcast.517), channel_id=1, replica_groups=mesh['sp_0'=8,'sp_1'=4,'sp_2'=2,'tp'=4] {'tp'}, dimensions={0} | all-to-all | bytes 1048576 | tf_op jit(solution)/shard_map/all_to_all | solution.py:67
  (325 shorter events, 78.5 us)
Async XLA Ops:
  6.5 142.2 %copy-start = (bf16[256,2048]{1,0:T(8,128)(2,1)S(1)}, bf16[256,2048]{1,0:T(8,128)(2,1)}, u32[]{:S(2)}) copy-start(bf16[256,2048]{1,0:T(8,128)(2,1)} %param.28) | copy-start | bytes 3145732
  6.5 174.9 %all-gather.9.cloned.1.call-start = ((), (), s32[]{:S(2)}) async-start(), calls=%async_computation.4 | async-start | bytes 11714560 | tf_op jit(solution)/shard_map/all_gather | solution.py:15
  8.3 176.9 %all-gather.11.cloned.1.call-start = ((), (), s32[]{:S(2)}) async-start(), calls=%async_computation.5 | async-start | bytes 5857280 | tf_op jit(solution)/shard_map/all_gather | solution.py:104
  13.9 7.3 %copy-start.4 = (f32[128,16]{0,1:T(8,128)S(1)}, f32[128,16]{0,1:T(8,128)}, u32[]{:S(2)}) copy-start(f32[128,16]{0,1:T(8,128)} %param.20) | copy-start | bytes 24580
  138.9 9.2 %copy-start.3 = (bf16[16,16,64]{2,1,0:T(8,128)(2,1)S(1)}, bf16[16,16,64]{2,1,0:T(8,128)(2,1)}, u32[]{:S(2)}) copy-start(bf16[16,16,64]{2,1,0:T(8,128)(2,1)} %param.26) | copy-start | bytes 98308
  140.3 8.4 %copy-start.1 = (bf16[128,256]{1,0:T(8,128)(2,1)S(1)}, bf16[128,256]{1,0:T(8,128)(2,1)}, u32[]{:S(2)}) copy-start(bf16[128,256]{1,0:T(8,128)(2,1)} %param.18) | copy-start | bytes 196612
  144.9 2.9 %copy-start.7 = (bf16[16,16,64]{2,1,0:T(8,128)(2,1)S(1)}, bf16[16,16,64]{2,1,0:T(8,128)(2,1)}, u32[]{:S(2)}) copy-start(bf16[16,16,64]{2,1,0:T(8,128)(2,1)} %param.25) | copy-start | bytes 98308
  145.8 2.9 %copy-start.5 = (f32[256]{0:T(256)S(1)}, f32[256]{0:T(256)}, u32[]{:S(2)}) copy-start(f32[256]{0:T(256)} %param.27) | copy-start | bytes 3076
  145.8 15.7 %copy-start.2 = (bf16[128,512]{1,0:T(8,128)(2,1)S(1)}, bf16[128,512]{1,0:T(8,128)(2,1)}, u32[]{:S(2)}) copy-start(bf16[128,512]{1,0:T(8,128)(2,1)} %param.29) | copy-start | bytes 393220
  145.9 19.6 %copy-start.6 = (bf16[512]{0:T(512)(128)(2,1)S(1)}, bf16[512]{0:T(512)(128)(2,1)}, u32[]{:S(2)}) copy-start(bf16[512]{0:T(512)(128)(2,1)} %param.30) | copy-start | bytes 3076
  162.2 8.4 %all-to-all-start.1 = ((f32[4,1,128]{2,1,0:T(1,128)}), f32[4,1,128]{2,1,0:T(1,128)S(1)}, u32[]{:S(2)}, u32[]{:S(2)}) async-start(f32[4,1,128]{2,1,0:T(1,128)} %broadcast_in_dim.17), calls=%async_computation.1 | async-start | bytes 4096 | tf_op jit(solution)/shard_map/all_to_all | solution.py:73
Sparse Core Ops, SparseCore 0:
  10.1 89.4 all-gather.8
  102.3 76.9 all-gather.10
where the time goes:
time: 214 us; the launch traced here: 210 us
  local copies, waits for them, and re-layouts  83.2 us (39%)
  blocking collectives  75.3 us (35%)
  other arithmetic  14.8 us (7%)
  between operations  13.9 us (6%)
  matrix products  13.4 us (6%)
  waiting for transfers between devices  5.89 us (3%)
  starting transfers between devices  3.27 us (2%)
    all_gather x3, blocking collectives, gathered_once(): both, at, found = (lax.all_gather(jnp.concatenate(lines), axis), 0, {})  42 us
    slice x64, local copies, waits for them, and re-layouts, advance(): carry = combine(carry, tuple((member[offset] for member in block)))  37 us
    all_to_all x2, blocking collectives, sent_and_summed(): pieces = lax.all_to_all(cut_along(x, dim, count), axis, 0, 0, tiled=True)  22.8 us
    dynamic_update_slice x32, local copies, waits for them, and re-layouts, local_states(): lax.scan(advance, (unity, nothing, nothing, nothing), blocks)  20.1 us
    all_to_all x1, blocking collectives, copy_for_each(): lax.all_to_all(jnp.broadcast_to(x[None], (count, *x.shape)), axis, 0, 0,...  10.5 us
    reshape x4, local copies, waits for them, and re-layouts, local_states(): return (finals, tuple((member.reshape(length, flat) for member in stacked)))  7.26 us
    dot_general x1, matrix products, local(): down_terms = jnp.dot(hidden, down_full, preferred_element_type=jnp.float32)  7.2 us
    squeeze x34, local copies, waits for them, and re-layouts, prefix_by_axis(): subtotal = combine(subtotal, jax.tree.map(lambda part: part[k], pieces))  5.93 us
  transfers between devices with their start and end apart: 3, of which 1 were waited for; matrix products, arithmetic and copies ran while one was open for 48% of the time, Pallas kernels for 0%

commit v1 on v0

v1 whole, which is shorter than its diff:
```python
import functools

import jax
import jax.numpy as jnp
from jax import lax
from jax.experimental import pallas as pl
from jax.experimental.pallas import tpu as pltpu
from jax.sharding import Mesh
from jax.sharding import PartitionSpec as P

SP = ("sp_0", "sp_1", "sp_2")
EPS = 1e-06
CHUNKS = 8
F32, BF16 = jnp.float32, jnp.bfloat16
EXACT = lax.Precision.HIGHEST
TO_LAST = (((1,), (1,)), ((), ()))


def iota(shape, dim):
    return lax.broadcasted_iota(jnp.int32, shape, dim)


def ones_where(mask, dtype):
    return jnp.where(mask, 1.0, 0.0).astype(dtype)


def exact_dot(a, b):
    return jnp.dot(a, b, precision=EXACT, preferred_element_type=F32)


def dot(a, b):
    return jnp.dot(a, b, preferred_element_type=F32)


def in_three(x):
    first = x.astype(BF16)
    rest = x - first.astype(F32)
    second = rest.astype(BF16)
    third = (rest - second.astype(F32)).astype(BF16)
    return first, second, third


def token_order(length):
    run = length // CHUNKS
    row, col = iota((length, length), 0), iota((length, length), 1)
    return (row % CHUNKS) * run + row // CHUNKS == col


def small_turn(angle):
    turns = jnp.floor(angle * 0.6366197723675814 + 0.5)
    rest = angle - turns * 1.5703125
    rest = rest - turns * 4.837512969970703e-4
    rest = rest - turns * 7.549789948768648e-8
    sq = rest * rest
    sine = rest + rest * sq * (-1.6666654611e-1 + sq * (8.3321608736e-3 - sq * 1.9515295891e-4))
    drop = sq * (-0.5 + sq * (4.166664568298827e-2 + sq * (-1.388731625493765e-3 + sq * 2.443315711809948e-5)))
    quarter = turns.astype(jnp.int32) & 3
    odd = (quarter & 1) == 1
    cosine = drop + 1.0
    sin_out = jnp.where(odd, cosine, sine)
    sin_out = jnp.where(quarter >= 2, -sin_out, sin_out)
    cos_out = jnp.where(odd, sine, cosine)
    cos_out = jnp.where((quarter == 1) | (quarter == 2), -cos_out, cos_out)
    return sin_out, jnp.where(quarter == 0, drop, cos_out - 1.0)


def shrink_minus_one(x):
    u = -x
    tail = 1 / 24 + u * (1 / 120 + u * (1 / 720 + u * (1 / 5040)))
    return u * (1.0 + u * (0.5 + u * (1 / 6 + u * tail)))


def whole_turn(angle):
    sine, cosine_minus = small_turn(angle)
    return sine, cosine_minus + 1.0


def scan_kernel(
    sig_ref, step_ref, forget_ref, damp_ref, freq_ref, inre_ref, inim_ref,
    lre_ref, lim_ref, pre_ref, pim_ref, chunk_ref, send_ref, rates_ref,
    src_ref, stp_ref, kp_ref, rows_ref, last_ref,
):
    length, groups = step_ref.shape
    states = damp_ref.shape[1]
    flat = groups * states
    width = sig_ref.shape[1] // groups
    run = length // CHUNKS
    order = token_order(length)
    sig = dot(ones_where(order, BF16), sig_ref[...]).astype(BF16)
    order32 = ones_where(order, F32)
    step_log, forget_log = step_ref[...], forget_ref[...]
    step = jnp.exp(step_log)
    spread = ones_where(iota((groups, flat), 0) == iota((groups, flat), 1) // states, F32)
    stp_ref[...] = exact_dot(exact_dot(order32, step), spread)
    kp_ref[...] = exact_dot(exact_dot(order32, jnp.exp(forget_log)), spread)
    tile = ones_where(iota((states, flat), 0) == iota((states, flat), 1) % states, F32)
    damp = jnp.sum(exact_dot(damp_ref[...], tile) * spread, axis=0, keepdims=True)
    freq = jnp.sum(exact_dot(freq_ref[...], tile) * spread, axis=0, keepdims=True)
    rates_ref[0:1, :] = damp
    rates_ref[1:2, :] = freq
    inverse = 1.0 / (damp * damp + freq * freq)
    rows_ref[0:1, :] = damp
    rows_ref[1:2, :] = freq
    rows_ref[2:3, :] = damp * inverse
    rows_ref[3:4, :] = freq * inverse
    tile_c = ones_where(iota((width, groups * width), 0) == iota((width, groups * width), 1) % width, BF16)
    own = iota((flat, groups * width), 0) // states == iota((flat, groups * width), 1) // width
    for part, ref in enumerate((inre_ref, inim_ref)):
        wide = jnp.where(own, dot(ref[...], tile_c), 0.0).astype(BF16)
        src_ref[:, part * flat : (part + 1) * flat] = lax.dot_general(sig, wide, TO_LAST, preferred_element_type=F32)

    def lanes(block, carry):
        at = pl.multiple_of(block * 128, 128)
        here = pl.ds(at, 128)
        shape = (CHUNKS, 128)
        d = jnp.broadcast_to(rows_ref[0:1, here], shape)
        w = jnp.broadcast_to(rows_ref[1:2, here], shape)
        wd = jnp.broadcast_to(rows_ref[2:3, here], shape)
        wf = jnp.broadcast_to(rows_ref[3:4, here], shape)
        p_re, p_im = jnp.ones(shape, F32), jnp.zeros(shape, F32)
        l_re, l_im = jnp.zeros(shape, F32), jnp.zeros(shape, F32)
        for i in range(run):
            rows = pl.ds(i * CHUNKS, CHUNKS)
            s = stp_ref[rows, here]
            keep = kp_ref[rows, here]
            sine, cos_less = small_turn(w * s)
            less = shrink_minus_one(d * s)
            mag = less + 1.0
            z_less = less + mag * cos_less
            z_im = mag * sine
            f_re = z_im * wf - z_less * wd
            f_im = -(z_im * wd + z_less * wf)
            s_re = src_ref[rows, here]
            s_im = src_ref[rows, pl.ds(pl.multiple_of(at + flat, 128), 128)]
            a_re = keep * (z_less + 1.0)
            a_im = keep * z_im
            l_re, l_im = (
                a_re * l_re - a_im * l_im + (f_re * s_re - f_im * s_im),
                a_re * l_im + a_im * l_re + (f_re * s_im + f_im * s_re),
            )
            p_re, p_im = a_re * p_re - a_im * p_im, a_re * p_im + a_im * p_re
            lre_ref[rows, here] = l_re
            lim_ref[rows, here] = l_im
            pre_ref[rows, here] = p_re
            pim_ref[rows, here] = p_im
        sub = iota(shape, 0)

        def earlier(value, by, fill):
            return jnp.where(sub >= by, pltpu.roll(value, by, 0), fill)

        for by in (1, 2, 4):
            q_re, q_im = earlier(p_re, by, 1.0), earlier(p_im, by, 0.0)
            m_re, m_im = earlier(l_re, by, 0.0), earlier(l_im, by, 0.0)
            l_re, l_im = p_re * m_re - p_im * m_im + l_re, p_re * m_im + p_im * m_re + l_im
            p_re, p_im = p_re * q_re - p_im * q_im, p_re * q_im + p_im * q_re
        chunk_ref[0:8, here] = earlier(p_re, 1, 1.0)
        chunk_ref[8:16, here] = earlier(p_im, 1, 0.0)
        chunk_ref[16:24, here] = earlier(l_re, 1, 0.0)
        chunk_ref[24:32, here] = earlier(l_im, 1, 0.0)
        last_ref[0:1, here] = l_re[7:8, :]
        last_ref[1:2, here] = l_im[7:8, :]
        return carry

    lax.fori_loop(0, flat // 128, lanes, 0)
    sums = in_three(jnp.sum(step, axis=0, keepdims=True)) + in_three(jnp.sum(forget_log, axis=0, keepdims=True))
    third = jnp.zeros((1, flat), F32)
    for k, piece in enumerate(sums):
        third = third + dot(piece, ones_where(iota((groups, flat), 0) == iota((groups, flat), 1) - k * groups, BF16))
    send_ref[:, 0:flat] = last_ref[0:1, :].astype(BF16)
    send_ref[:, flat : 2 * flat] = last_ref[1:2, :].astype(BF16)
    send_ref[:, 2 * flat : 3 * flat] = third.astype(BF16)


def local_scan(signal, step_log, forget_log, damping, freq, in_re, in_im):
    length, groups = step_log.shape
    states = damping.shape[1]
    flat = groups * states
    wide = jax.ShapeDtypeStruct((length, flat), F32)
    return pl.pallas_call(
        scan_kernel,
        out_shape=(
            wide, wide, wide, wide,
            jax.ShapeDtypeStruct((32, flat), F32),
            jax.ShapeDtypeStruct((1, 3 * flat), BF16),
            jax.ShapeDtypeStruct((2, flat), F32),
        ),
        scratch_shapes=[
            pltpu.VMEM((length, 2 * flat), F32),
            pltpu.VMEM((length, flat), F32),
            pltpu.VMEM((length, flat), F32),
            pltpu.VMEM((8, flat), F32),
            pltpu.VMEM((8, flat), F32),
        ],
        compiler_params=pltpu.CompilerParams(vmem_limit_bytes=24 * 2**20),
        cost_estimate=pl.CostEstimate(flops=4 * 10**9, bytes_accessed=3 * 2**20, transcendentals=0),
        name="local_scan",
    )(
        signal, step_log, forget_log, damping, freq,
        in_re.reshape(flat, -1), in_im.reshape(flat, -1),
    )


def readout_kernel(
    all_ref, lre_ref, lim_ref, pre_ref, pim_ref, chunk_ref, rates_ref, sig_ref, outre_ref, outim_ref, skip_ref, wout_ref,
    part_ref,
    are_ref, aim_ref, bre_ref, bim_ref, st_ref, wide_ref,
    *, sizes,
):
    length, flat = lre_ref.shape
    devices = all_ref.shape[0]
    outs, states = outre_ref.shape
    groups = flat // states
    width = outs // groups
    n_z = sizes[0]
    inner = devices // n_z
    row, col = iota((groups * 8, flat), 0), iota((groups * 8, flat), 1)
    own = row % groups == col // states
    sums = all_ref[:, 2 * flat : 2 * flat + 128]
    step = dot(sums, ones_where(own & (row < 3 * groups), BF16))
    forget = dot(sums, ones_where(own & (row >= 3 * groups) & (row < 6 * groups), BF16))
    sine, cosine = whole_turn(rates_ref[1:2, :] * step)
    mag = jnp.exp(forget - rates_ref[0:1, :] * step)
    me = (lax.axis_index("sp_0") * sizes[1] + lax.axis_index("sp_1")) * sizes[2] + lax.axis_index("sp_2")
    place = (iota((devices, flat), 0) % n_z) * inner + iota((devices, flat), 0) // n_z
    before = place < me
    are_ref[...] = jnp.where(before, mag * cosine, 1.0)
    aim_ref[...] = jnp.where(before, mag * sine, 0.0)
    bre_ref[...] = jnp.where(before, all_ref[:, 0:flat].astype(F32), 0.0)
    bim_ref[...] = jnp.where(before, all_ref[:, flat : 2 * flat].astype(F32), 0.0)
    p_re, p_im = jnp.ones((n_z, flat), F32), jnp.zeros((n_z, flat), F32)
    l_re, l_im = jnp.zeros((n_z, flat), F32), jnp.zeros((n_z, flat), F32)
    for i in range(inner):
        rows = pl.ds(i * n_z, n_z)
        a_re, a_im = are_ref[rows, :], aim_ref[rows, :]
        l_re, l_im = a_re * l_re - a_im * l_im + bre_ref[rows, :], a_re * l_im + a_im * l_re + bim_ref[rows, :]
        p_re, p_im = a_re * p_re - a_im * p_im, a_re * p_im + a_im * p_re
    by = 1
    while by < n_z:
        q_re, q_im = pltpu.roll(p_re, by, 0), pltpu.roll(p_im, by, 0)
        m_re, m_im = pltpu.roll(l_re, by, 0), pltpu.roll(l_im, by, 0)
        l_re, l_im = p_re * m_re - p_im * m_im + l_re, p_re * m_im + p_im * m_re + l_im
        p_re, p_im = p_re * q_re - p_im * q_im, p_re * q_im + p_im * q_re
        by *= 2
    b_re = jnp.broadcast_to(l_re[n_z - 1 : n_z, :], (8, flat))
    b_im = jnp.broadcast_to(l_im[n_z - 1 : n_z, :], (8, flat))
    c_re, c_im = chunk_ref[0:8, :], chunk_ref[8:16, :]
    first_re = c_re * b_re - c_im * b_im + chunk_ref[16:24, :]
    first_im = c_re * b_im + c_im * b_re + chunk_ref[24:32, :]
    for i in range(length // 16):
        pair_re, pair_im = [], []
        for h in range(2):
            rows = pl.ds(i * 16 + h * 8, 8)
            q_re, q_im = pre_ref[rows, :], pim_ref[rows, :]
            pair_re.append(lre_ref[rows, :] + q_re * first_re - q_im * first_im)
            pair_im.append(lim_ref[rows, :] + q_re * first_im + q_im * first_re)
        rows = pl.ds(i * 16, 16)
        st_ref[rows, 0:flat] = jnp.concatenate(pair_re, axis=0).astype(BF16)
        st_ref[rows, flat : 2 * flat] = jnp.concatenate(pair_im, axis=0).astype(BF16)
    tile = ones_where(iota((states, flat), 0) == iota((states, flat), 1) % states, BF16)
    mine = iota((outs, flat), 0) // width == iota((outs, flat), 1) // states
    wide_ref[:, 0:flat] = jnp.where(mine, dot(outre_ref[...], tile), 0.0).astype(BF16)
    wide_ref[:, flat : 2 * flat] = jnp.where(mine, -dot(outim_ref[...], tile), 0.0).astype(BF16)
    order = ones_where(token_order(length), BF16)
    sig = dot(order, sig_ref[...])
    value = lax.dot_general(st_ref[...], wide_ref[...], TO_LAST, preferred_element_type=F32) + skip_ref[...] * sig
    cube = 0.7978845608028654 * (value + 0.044715 * (value * value * value))
    mixed = (0.5 * value * (1.0 + jnp.tanh(cube))).astype(BF16)
    back = lax.dot_general(order, mixed, (((0,), (0,)), ((), ())), preferred_element_type=F32).astype(BF16)
    n_part, cols = part_ref.shape[0], part_ref.shape[2]
    for k in range(n_part):
        part_ref[k] = dot(back, wout_ref[:, k * cols : (k + 1) * cols]).astype(BF16)


def readout(gathered, scanned, signal, out_re, out_im, skip, w_out, n_tp, sizes):
    lre, lim, pre, pim, chunk, rates = scanned
    length, flat = lre.shape
    devices = gathered.shape[0]
    states = out_re.shape[2]
    outs = out_re.shape[0] * out_re.shape[1]
    model = w_out.shape[1]
    return pl.pallas_call(
        functools.partial(readout_kernel, sizes=sizes),
        out_shape=jax.ShapeDtypeStruct((n_tp, length, model // n_tp), BF16),
        scratch_shapes=[pltpu.VMEM((devices, flat), F32)] * 4
        + [pltpu.VMEM((length, 2 * flat), BF16), pltpu.VMEM((outs, 2 * flat), BF16)],
        compiler_params=pltpu.CompilerParams(vmem_limit_bytes=24 * 2**20),
        cost_estimate=pl.CostEstimate(flops=4 * 10**9, bytes_accessed=4 * 2**20, transcendentals=0),
        name="readout",
    )(
        gathered, lre, lim, pre, pim, chunk, rates, signal,
        out_re.reshape(outs, states), out_im.reshape(outs, states), skip.reshape(1, outs), w_out,
    )


def middle_kernel(part_ref, res_ref, gain_ref, mid_ref):
    length = res_ref.shape[0]
    total = res_ref[...].astype(F32)
    added = part_ref[0].astype(F32)
    for k in range(1, part_ref.shape[0]):
        added = added + part_ref[k].astype(F32)
    mid_ref[0:length, :] = (total + added).astype(BF16)
    extra = mid_ref.shape[0] - length
    mid_ref[length:, :] = jnp.broadcast_to(gain_ref[...], (extra, gain_ref.shape[1]))


def middle_of(parts, residual, gain):
    length, cols = residual.shape
    return pl.pallas_call(
        middle_kernel,
        out_shape=jax.ShapeDtypeStruct((length + 16, cols), BF16),
        cost_estimate=pl.CostEstimate(flops=10**6, bytes_accessed=2**20, transcendentals=0),
        name="middle",
    )(parts, residual, gain.reshape(1, cols))


def ffn_kernel(mid_ref, wg_ref, wu_ref, wd_ref, out_ref, norm_ref, sum_ref):
    n_tp, rows, cols = mid_ref.shape
    length = rows - 16
    at = pl.program_id(0)

    @pl.when(at == 0)
    def _():
        squares = jnp.zeros((length, 1), F32)
        for k in range(n_tp):
            m = mid_ref[k, 0:length, :].astype(F32)
            squares = squares + jnp.sum(m * m, axis=1, keepdims=True)
        scale = lax.rsqrt(squares / (n_tp * cols) + EPS)
        for k in range(n_tp):
            m = mid_ref[k, 0:length, :].astype(F32)
            gain = mid_ref[k, length : length + 1, :].astype(F32)
            norm_ref[:, k * cols : (k + 1) * cols] = (m * scale * gain).astype(BF16)
        sum_ref[...] = jnp.zeros_like(sum_ref)

    gate = dot(norm_ref[...], wg_ref[...])
    up = dot(norm_ref[...], wu_ref[...])
    hidden = (gate / (1.0 + jnp.exp(-gate)) * up).astype(BF16)
    sum_ref[...] += lax.dot_general(hidden, wd_ref[...], TO_LAST, preferred_element_type=F32)

    @pl.when(at == pl.num_programs(0) - 1)
    def _():
        for k in range(n_tp):
            out_ref[k] = sum_ref[:, k * cols : (k + 1) * cols].astype(BF16)


def ffn(mid, weights, hidden):
    n_tp, rows, cols = mid.shape
    model = n_tp * cols
    block = 128
    steps = hidden // block
    return pl.pallas_call(
        ffn_kernel,
        grid=(steps,),
        in_specs=[
            pl.BlockSpec((n_tp, rows, cols), lambda i: (0, 0, 0)),
            pl.BlockSpec((model, block), lambda i: (0, i)),
            pl.BlockSpec((model, block), lambda i: (0, i + steps)),
            pl.BlockSpec((model, block), lambda i: (0, i + 2 * steps)),
        ],
        out_specs=pl.BlockSpec((n_tp, rows - 16, cols), lambda i: (0, 0, 0)),
        out_shape=jax.ShapeDtypeStruct((n_tp, rows - 16, cols), BF16),
        scratch_shapes=[pltpu.VMEM((rows - 16, model), BF16), pltpu.VMEM((rows - 16, model), F32)],
        compiler_params=pltpu.CompilerParams(vmem_limit_bytes=32 * 2**20),
        cost_estimate=pl.CostEstimate(flops=4 * 10**9, bytes_accessed=18 * 2**20, transcendentals=0),
        name="ffn",
    )(mid, weights, weights, weights)


def copy_for_each(x, axis, count):
    return lax.all_to_all(jnp.broadcast_to(x[None], (count, *x.shape)), axis, 0, 0, tiled=True)


def local(
    signal, step_log, forget_log, damping, freq, in_re, in_im, out_re, out_im, skip,
    w_out, residual, norm_gain, w_gate, w_up, w_down,
):
    sizes = tuple(lax.axis_size(a) for a in SP)
    n_sp = sizes[0] * sizes[1] * sizes[2]
    n_tp = lax.axis_size("tp")
    hidden = w_gate.shape[1]
    together = jnp.concatenate([w_gate, w_up, w_down.T], axis=1)
    weights = lax.all_gather(together, SP, axis=0, tiled=True)
    *scanned, send, rates = local_scan(signal, step_log, forget_log, damping, freq, in_re, in_im)
    gathered = copy_for_each(send, ("sp_1", "sp_2", "sp_0"), n_sp).reshape(n_sp, -1)
    parts = readout(gathered, (*scanned, rates), signal, out_re, out_im, skip, w_out, n_tp, sizes)
    parts = lax.all_to_all(parts, "tp", 0, 0, tiled=True)
    mid = middle_of(parts, residual, norm_gain)
    everyone = lax.all_gather(mid, "tp")
    down = ffn(everyone, weights, hidden)
    down = lax.all_to_all(down, "tp", 0, 0, tiled=True)
    own = mid[: residual.shape[0]].astype(F32)
    return (own + 0.5 * jnp.sum(down.astype(F32), axis=0)).astype(BF16)


def solution(mesh):
    torus = Mesh(mesh.devices.reshape(8, 4, 2, mesh.shape["tp"]), ("sp_0", "sp_1", "sp_2", "tp"))
    return jax.shard_map(
        local,
        mesh=torus,
        in_specs=(
            P(SP, "tp"), P(SP, "tp"), P(SP, "tp"),
            P("tp", None), P("tp", None),
            P("tp", None, None), P("tp", None, None), P("tp", None, None), P("tp", None, None),
            P("tp"), P("tp", None), P(SP, "tp"), P("tp"),
            P(SP, "tp"), P(SP, "tp"), P("tp", SP),
        ),
        out_specs=P(SP, "tp"),
        check_vma=False,
    )
```

time: 214 us -> 156 us (0.73)
  local copies, waits for them, and re-layouts: 83.2 us -> 24.5 us
  waiting for transfers between devices: 5.89 us -> 26.7 us
  Pallas kernels: 0 us -> 20.1 us
  blocking collectives: 75.3 us -> 57.1 us
  matrix products: 13.4 us -> 0 us
  other arithmetic: 14.8 us -> 7.28 us
    slice x66 -> x0, local copies, waits for them, and re-layouts: 37.2 us -> none  [the longest x64 37 us: advance(): carry = combine(carry, tuple((member[offset] for member in block)))]
    all_gather x3 -> x1, blocking collectives: 42 us -> 13.3 us  [local(): everyone = lax.all_gather(mid, 'tp')]
    unnamed x18 -> x39, local copies, waits for them, and re-layouts: 1.1 us -> 22.1 us
    dynamic_update_slice x32 -> x0, local copies, waits for them, and re-layouts: 20.1 us -> none  [local_states(): lax.scan(advance, (unity, nothing, nothing, nothing), blocks)]
    pallas_call x0 -> x4, Pallas kernels: none -> 20.1 us  [the longest x1 11 us: ffn(): pl.pallas_call(ffn_kernel, grid=(steps,), in_specs=[pl.BlockSpec((n_tp, r...]
    all_to_all x1, blocking collectives: 10.5 us -> 29.8 us  [copy_for_each(): lax.all_to_all(jnp.broadcast_to(x[None], (count, *x.shape)), axis, 0, 0,...]
    all_gather x2 -> x1, waiting for transfers between devices: 0.02 us -> 18.2 us  [local(): weights = lax.all_gather(together, SP, axis=0, tiled=True)]
    dot_general x6 -> x0, matrix products: 13.4 us -> none  [the longest x1 7.2 us: local(): down_terms = jnp.dot(hidden, down_full, preferred_element_type=jnp.float32)]
  transfers between devices with their start and end apart: 3 -> 2, of which waited for: 1 -> 2; matrix products, arithmetic and copies ran while one was open for 48% -> 11% of each run, Pallas kernels for 0% -> 6%
where the time goes in v1:
time: 156 us; the launch traced here: 154 us
  blocking collectives  57.1 us (37%)
  waiting for transfers between devices  26.7 us (17%)
  local copies, waits for them, and re-layouts  24.5 us (16%)
  Pallas kernels  20.1 us (13%)
  between operations  13.5 us (9%)
  other arithmetic  7.28 us (5%)
  starting transfers between devices  4.59 us (3%)
    all_to_all x1, blocking collectives, copy_for_each(): lax.all_to_all(jnp.broadcast_to(x[None], (count, *x.shape)), axis, 0, 0,...  29.8 us
    unnamed x39, local copies, waits for them, and re-layouts  22.1 us
    all_gather x1, waiting for transfers between devices, local(): weights = lax.all_gather(together, SP, axis=0, tiled=True)  18.2 us
    all_to_all x1, blocking collectives, local(): down = lax.all_to_all(down, 'tp', 0, 0, tiled=True)  14 us
    all_gather x1, blocking collectives, local(): everyone = lax.all_gather(mid, 'tp')  13.3 us
    pallas_call x1, Pallas kernels, ffn(): pl.pallas_call(ffn_kernel, grid=(steps,), in_specs=[pl.BlockSpec((n_tp, r...  11 us
    all_to_all x1, waiting for transfers between devices, local(): parts = lax.all_to_all(parts, 'tp', 0, 0, tiled=True)  8.52 us
    broadcast_in_dim x1, other arithmetic, copy_for_each(): jnp.broadcast_to(x[None], (count, *x.shape))  4.69 us
  transfers between devices with their start and end apart: 2, of which 2 were waited for; matrix products, arithmetic and copies ran while one was open for 11% of the time, Pallas kernels for 6%

profile of v1, /device:TPU:2, one launch (start us, length us, event | category | flops | bytes accessed | tf_op | source)
XLA Modules:
  0.0 153.9 jit_solution(17693268459427593306)
XLA Ops:
  6.6 1.8 %pad_maximum_fusion = bf16[32,4224]{1,0:T(8,128)(2,1)} fusion(bf16[32,1408]{1,0:T(8,128)(2,1)} %bitcast.17, bf16[32,1408]{1,0:T(8,128)(2,1)} %param.30, bf16[32,1408]{1,0:T(8,128)(2,1)} %param.29), kind=kLoop, calls=%fused_computation.2 | loop fusion | flops 811008 | bytes 540672 | tf_op jit(solution)/shard_map/concatenate | solution.py:380
  8.4 1.0 copy.25
  9.4 1.0 copy.26
  10.4 0.8 copy.27.step_ref
  12.0 0.8 copy-done.2
  14.3 4.4 %local_scan.1 = (f32[128,1024]{1,0:T(8,128)S(1)}, f32[128,1024]{1,0:T(8,128)S(1)}, f32[128,1024]{1,0:T(8,128)S(1)}, f32[128,1024]{1,0:T(8,128)S(1)}, f32[32,1024...) custom-call(bf16[128,256]{1,0:T(8,128)(2,1)S(1)} %copy-done.2, f32[128,16]{1,0:T(8,128)S(1)} %copy.27.step_ref, ...), custom_call_target="tpu_custom_call" | custom-call | flops 4000000000 | bytes 3145728 | tf_op jit(solution)/shard_map/local_scan/pallas_call | solution.py:179
  18.7 0.8 copy-done.9
  20.2 1.3 broadcast_in_dim.9
  22.1 4.7 %reduce.1 = bf16[64,3072]{1,0:T(8,128)(2,1)} reduce(bf16[64,1,3072]{2,1,0:T(2,128)(2,1)} %broadcast_in_dim.9, bf16[]{:T(256)} %broadcast.2), dimensions={1}, to_apply=%broadcast_in_dim.9.reduce_sub_computation | reduce | bytes 786434 | tf_op jit(solution)/shard_map/broadcast_in_dim | solution.py:369
  26.8 1.3 reshape.33
  28.1 29.8 %all_to_all.15 = bf16[64,2,1536]{2,1,0:T(2,128)(2,1)} all-to-all(bf16[64,2,1536]{2,1,0:T(2,128)(2,1)S(1)} %reshape.33), channel_id=1, replica_groups=mesh['sp_0'=8,'sp_1'=4,'sp_2'=2,'tp'=4] {'sp_1','sp_2','sp_0'}, dimensions={0} | all-to-all | bytes 786432 | tf_op jit(solution)/shard_map/all_to_all | solution.py:369
  57.9 3.5 %reshape.34 = bf16[64,1,3072]{2,1,0:T(2,128)(2,1)} reshape(bf16[64,2,1536]{2,1,0:T(2,128)(2,1)} %all_to_all.15) | data formatting | bytes 786432
  61.4 1.3 copy.31
  62.8 1.0 copy-done.10
  63.8 0.9 copy-done.12
  64.7 2.8 %readout.1 = bf16[4,128,512]{2,1,0:T(8,128)(2,1)} custom-call(bf16[64,3072]{1,0:T(8,128)(2,1)S(1)} %bitcast.11, f32[128,1024]{1,0:T(8,128)S(1)} %get-tuple-element.13.lre_ref, f32[128,1024]{1,0:T(8,128)S(1)} %get-tuple-element.14.lim_ref, f32[128,1024]{1,0:T(8,128)S(1)} %get-tuple-element.15.pre_ref, f32[128,1024]{1,0:T(8,128)S(1)} %copy-done.10, ...), custom_call_target="tpu_custom_call" | custom-call | flops 4000000000 | bytes 4194304 | tf_op jit(solution)/shard_map/readout/pallas_call | solution.py:281
  67.5 4.6 %all-to-all-start.1 = ((bf16[4,128,512]{2,1,0:T(8,128)(2,1)}), bf16[4,128,512]{2,1,0:T(8,128)(2,1)S(1)}, u32[]{:S(2)}, u32[]{:S(2)}) async-start(bf16[4,128,512]{2,1,0:T(8,128)(2,1)} %readout.1), calls=%async_computation.1 | async-start | bytes 1048576 | tf_op jit(solution)/shard_map/all_to_all | solution.py:385
  72.7 8.5 %all-to-all-done.1.part_ref = bf16[4,128,512]{2,1,0:T(8,128)(2,1)S(1)} async-done(((bf16[4,128,512]{2,1,0:T(8,128)(2,1)}), bf16[4,128,512]{2,1,0:T(8,128)(2,1)S(1)}, u32[]{:S(2)}, u32[]{:S(2)}) %all-to-all-start.1) | async-done | bytes 524320 | tf_op jit(solution)/shard_map/all_to_all | solution.py:385
  82.0 1.9 %middle.1 = bf16[144,512]{1,0:T(8,128)(2,1)} custom-call(bf16[4,128,512]{2,1,0:T(8,128)(2,1)} %copy-done.13, bf16[128,512]{1,0:T(8,128)(2,1)} %res_ref.1, bf16[1,512]{1,0:T(2,128)(2,1)} %reshape.30.gain_ref), custom_call_target="tpu_custom_call" | custom-call | flops 1000000 | bytes 1048576 | tf_op jit(solution)/shard_map/middle/pallas_call | solution.py:308
  83.9 13.3 %all-gather = bf16[576,512]{1,0:T(8,128)(2,1)S(1)} all-gather(bf16[144,512]{1,0:T(8,128)(2,1)} %middle.1), channel_id=2, replica_groups=mesh['sp_0'=8,'sp_1'=4,'sp_2'=2,'tp'=4] {'tp'}, dimensions={0}, use_global_device_ids=true | all-gather | bytes 737280 | tf_op jit(solution)/shard_map/all_gather | solution.py:387
  97.2 18.2 %all-gather.3.cloned.1.call-done.wg_ref.wu_ref.wd_ref = bf16[2048,4224]{1,0:T(8,128)(2,1)} async-done(((bf16[32,4224]{1,0:T(8,128)(2,1)}), bf16[2048,4224]{1,0:T(8,128)(2,1)}) %all-gather.3.cloned.1.call-update) | async-done | bytes 17301520 | tf_op jit(solution)/shard_map/all_gather | solution.py:381
  115.4 5.9 %copy-done = bf16[2048,4224]{1,0:T(8,128)(2,1)S(1)} copy-done((bf16[2048,4224]{1,0:T(8,128)(2,1)S(1)}, bf16[2048,4224]{1,0:T(8,128)(2,1)}, u32[]{:S(2)}) %copy-start) | copy-done | bytes 17301528
  121.3 11.0 %ffn.1 = bf16[4,128,512]{2,1,0:T(8,128)(2,1)S(1)} custom-call(bf16[4,144,512]{2,1,0:T(8,128)(2,1)S(1)} %bitcast.10, bf16[2048,4224]{1,0:T(8,128)(2,1)S(1)} %copy-done, bf16[2048,4224]{1,0:T(8,128)(2,1)S(1)} %copy-done, bf16[2048,4224]{1,0:T(8,128)(2,1)S(1)} %copy-done), custom_call_target="tpu_custom_call" | custom-call | flops 4000000000 | bytes 18874368 | tf_op jit(solution)/shard_map/ffn/pallas_call | solution.py:350
  132.3 14.0 %all_to_all.16 = bf16[4,128,512]{2,1,0:T(8,128)(2,1)S(1)} all-to-all(bf16[4,128,512]{2,1,0:T(8,128)(2,1)S(1)} %ffn.1), channel_id=1, replica_groups=mesh['sp_0'=8,'sp_1'=4,'sp_2'=2,'tp'=4] {'tp'}, dimensions={0} | all-to-all | bytes 1048576 | tf_op jit(solution)/shard_map/all_to_all | solution.py:389
  (35 shorter events, 5.7 us)
Async XLA Ops:
  6.5 56.2 %copy-start.3 = (bf16[128,256]{1,0:T(8,128)(2,1)S(1)}, bf16[128,256]{1,0:T(8,128)(2,1)}, u32[]{:S(2)}) copy-start(bf16[128,256]{1,0:T(8,128)(2,1)} %sig_ref.3) | copy-start | bytes 196612
  6.5 56.2 %copy-start.4 = (bf16[16,16,64]{2,1,0:T(8,128)(2,1)S(1)}, bf16[16,16,64]{2,1,0:T(8,128)(2,1)}, u32[]{:S(2)}) copy-start(bf16[16,16,64]{2,1,0:T(8,128)(2,1)} %param.23) | copy-start | bytes 98308
  6.5 56.2 %copy-start.5 = (bf16[16,16,64]{2,1,0:T(8,128)(2,1)S(1)}, bf16[16,16,64]{2,1,0:T(8,128)(2,1)}, u32[]{:S(2)}) copy-start(bf16[16,16,64]{2,1,0:T(8,128)(2,1)} %param.24) | copy-start | bytes 98308
  6.5 56.2 %copy-start.8 = (f32[256]{0:T(256)S(1)}, f32[256]{0:T(256)}, u32[]{:S(2)}) copy-start(f32[256]{0:T(256)} %param.25) | copy-start | bytes 3076
  6.5 56.2 %copy-start.1 = (bf16[256,2048]{1,0:T(8,128)(2,1)S(1)}, bf16[256,2048]{1,0:T(8,128)(2,1)}, u32[]{:S(2)}) copy-start(bf16[256,2048]{1,0:T(8,128)(2,1)} %wout_ref.1) | copy-start | bytes 3145732
  6.5 108.8 %all-gather.3.cloned.1.call-start = ((), (), s32[]{:S(2)}) async-start(), calls=%async_computation.3 | async-start | bytes 17571840 | tf_op jit(solution)/shard_map/all_gather | solution.py:381
  12.0 0.8 copy-start.2
  12.9 0.7 copy-start.6
  13.6 0.7 copy-start.7
  14.3 57.8 %copy-start.15 = (bf16[512]{0:T(512)(128)(2,1)S(1)}, bf16[512]{0:T(512)(128)(2,1)}, u32[]{:S(2)}) copy-start(bf16[512]{0:T(512)(128)(2,1)} %param.28) | copy-start | bytes 3076
  18.7 0.8 copy-start.9
  19.5 0.7 copy-start.11
  62.8 1.0 copy-start.10
  63.8 0.9 copy-start.12
  67.5 13.7 %all-to-all-start.1 = ((bf16[4,128,512]{2,1,0:T(8,128)(2,1)}), bf16[4,128,512]{2,1,0:T(8,128)(2,1)S(1)}, u32[]{:S(2)}, u32[]{:S(2)}) async-start(bf16[4,128,512]{2,1,0:T(8,128)(2,1)} %readout.1), calls=%async_computation.1 | async-start | bytes 1048576 | tf_op jit(solution)/shard_map/all_to_all | solution.py:385
  81.2 0.8 copy-start.13
  115.4 5.9 %copy-start = (bf16[2048,4224]{1,0:T(8,128)(2,1)S(1)}, bf16[2048,4224]{1,0:T(8,128)(2,1)}, u32[]{:S(2)}) copy-start(bf16[2048,4224]{1,0:T(8,128)(2,1)} %all-gather.3.cloned.1.call-done.wg_ref.wu_ref.wd_ref) | copy-start | bytes 51904516
  121.3 25.0 %copy-start.14 = (bf16[144,512]{1,0:T(8,128)(2,1)S(1)}, bf16[144,512]{1,0:T(8,128)(2,1)}, u32[]{:S(2)}) copy-start(bf16[144,512]{1,0:T(8,128)(2,1)} %middle.1) | copy-start | bytes 442372
Sparse Core Ops, SparseCore 0:
  10.1 105.2 all-gather.2

commit v2 on v1

v2 whole, which is shorter than its diff:
```python
import functools

import jax
import jax.numpy as jnp
from jax import lax
from jax.experimental import pallas as pl
from jax.experimental.pallas import tpu as pltpu
from jax.sharding import Mesh
from jax.sharding import PartitionSpec as P


SP = ("sp_0", "sp_1", "sp_2")
EPS = 1e-06
CHUNKS = 8
F32, BF16 = jnp.float32, jnp.bfloat16
EXACT = lax.Precision.HIGHEST
TO_LAST = (((1,), (1,)), ((), ()))


def iota(shape, dim):
    return lax.broadcasted_iota(jnp.int32, shape, dim)


def ones_where(mask, dtype):
    return jnp.where(mask, 1.0, 0.0).astype(dtype)


def exact_dot(a, b):
    return jnp.dot(a, b, precision=EXACT, preferred_element_type=F32)


def dot(a, b):
    return jnp.dot(a, b, preferred_element_type=F32)


def token_order(length):
    run = length // CHUNKS
    row, col = iota((length, length), 0), iota((length, length), 1)
    return (row % CHUNKS) * run + row // CHUNKS == col


def small_turn(angle):
    turns = jnp.floor(angle * 0.6366197723675814 + 0.5)
    rest = angle - turns * 1.5703125
    rest = rest - turns * 4.837512969970703e-4
    rest = rest - turns * 7.549789948768648e-8
    sq = rest * rest
    sine = rest + rest * sq * (-1.6666654611e-1 + sq * (8.3321608736e-3 - sq * 1.9515295891e-4))
    drop = sq * (-0.5 + sq * (4.166664568298827e-2 + sq * (-1.388731625493765e-3 + sq * 2.443315711809948e-5)))
    quarter = turns.astype(jnp.int32) & 3
    odd = (quarter & 1) == 1
    cosine = drop + 1.0
    sin_out = jnp.where(odd, cosine, sine)
    sin_out = jnp.where(quarter >= 2, -sin_out, sin_out)
    cos_out = jnp.where(odd, sine, cosine)
    cos_out = jnp.where((quarter == 1) | (quarter == 2), -cos_out, cos_out)
    return sin_out, jnp.where(quarter == 0, drop, cos_out - 1.0)


def shrink_minus_one(x):
    u = -x
    tail = 1 / 24 + u * (1 / 120 + u * (1 / 720 + u * (1 / 5040)))
    return u * (1.0 + u * (0.5 + u * (1 / 6 + u * tail)))


def scan_kernel(
    sig_ref, step_ref, forget_ref, damp_ref, freq_ref, inre_ref, inim_ref,
    all_ref, chunk_ref, send_ref,
    src_ref, stp_ref, kp_ref, rows_ref, last_ref,
):
    length, groups = step_ref.shape
    states = damp_ref.shape[1]
    flat = groups * states
    width = sig_ref.shape[1] // groups
    run = length // CHUNKS
    order = token_order(length)
    sig = dot(ones_where(order, BF16), sig_ref[...]).astype(BF16)
    order32 = ones_where(order, F32)
    step_log, forget_log = step_ref[...], forget_ref[...]
    step = jnp.exp(step_log)
    spread = ones_where(iota((groups, flat), 0) == iota((groups, flat), 1) // states, F32)
    stp_ref[...] = exact_dot(exact_dot(order32, step), spread)
    kp_ref[...] = exact_dot(exact_dot(order32, jnp.exp(forget_log)), spread)
    tile = ones_where(iota((states, flat), 0) == iota((states, flat), 1) % states, F32)
    damp = jnp.sum(exact_dot(damp_ref[...], tile) * spread, axis=0, keepdims=True)
    freq = jnp.sum(exact_dot(freq_ref[...], tile) * spread, axis=0, keepdims=True)
    inverse = 1.0 / (damp * damp + freq * freq)
    rows_ref[0:1, :] = damp
    rows_ref[1:2, :] = freq
    rows_ref[2:3, :] = damp * inverse
    rows_ref[3:4, :] = freq * inverse
    tile_c = ones_where(iota((width, groups * width), 0) == iota((width, groups * width), 1) % width, BF16)
    own = iota((flat, groups * width), 0) // states == iota((flat, groups * width), 1) // width
    for part, ref in enumerate((inre_ref, inim_ref)):
        wide = jnp.where(own, dot(ref[...], tile_c), 0.0).astype(BF16)
        src_ref[:, part * flat : (part + 1) * flat] = lax.dot_general(sig, wide, TO_LAST, preferred_element_type=F32)

    def lanes(block, carry):
        at = pl.multiple_of(block * 128, 128)
        here = pl.ds(at, 128)
        shape = (CHUNKS, 128)
        d = jnp.broadcast_to(rows_ref[0:1, here], shape)
        w = jnp.broadcast_to(rows_ref[1:2, here], shape)
        wd = jnp.broadcast_to(rows_ref[2:3, here], shape)
        wf = jnp.broadcast_to(rows_ref[3:4, here], shape)
        p_re, p_im = jnp.ones(shape, F32), jnp.zeros(shape, F32)
        l_re, l_im = jnp.zeros(shape, F32), jnp.zeros(shape, F32)
        for i in range(run):
            rows = pl.ds(i * CHUNKS, CHUNKS)
            s = stp_ref[rows, here]
            keep = kp_ref[rows, here]
            sine, cos_less = small_turn(w * s)
            less = shrink_minus_one(d * s)
            mag = less + 1.0
            z_less = less + mag * cos_less
            z_im = mag * sine
            f_re = z_im * wf - z_less * wd
            f_im = -(z_im * wd + z_less * wf)
            s_re = src_ref[rows, here]
            s_im = src_ref[rows, pl.ds(pl.multiple_of(at + flat, 128), 128)]
            a_re = keep * (z_less + 1.0)
            a_im = keep * z_im
            l_re, l_im = (
                a_re * l_re - a_im * l_im + (f_re * s_re - f_im * s_im),
                a_re * l_im + a_im * l_re + (f_re * s_im + f_im * s_re),
            )
            p_re, p_im = a_re * p_re - a_im * p_im, a_re * p_im + a_im * p_re
            for k, value in enumerate((l_re, l_im, p_re, p_im)):
                all_ref[pl.ds(k * length + i * CHUNKS, CHUNKS), here] = value
        sub = iota(shape, 0)

        def earlier(value, by, fill):
            return jnp.where(sub >= by, pltpu.roll(value, by, 0), fill)

        for by in (1, 2, 4):
            q_re, q_im = earlier(p_re, by, 1.0), earlier(p_im, by, 0.0)
            m_re, m_im = earlier(l_re, by, 0.0), earlier(l_im, by, 0.0)
            l_re, l_im = p_re * m_re - p_im * m_im + l_re, p_re * m_im + p_im * m_re + l_im
            p_re, p_im = p_re * q_re - p_im * q_im, p_re * q_im + p_im * q_re
        chunk_ref[0:8, here] = earlier(p_re, 1, 1.0)
        chunk_ref[8:16, here] = earlier(p_im, 1, 0.0)
        chunk_ref[16:24, here] = earlier(l_re, 1, 0.0)
        chunk_ref[24:32, here] = earlier(l_im, 1, 0.0)
        for k, value in enumerate((p_re, p_im, l_re, l_im)):
            last_ref[pl.ds(block + 8 * k, 1), :] = value[7:8, :]
        return carry

    lax.fori_loop(0, flat // 128, lanes, 0)
    for k in range(send_ref.shape[0]):
        send_ref[k] = last_ref[...]


def local_scan(signal, step_log, forget_log, damping, freq, in_re, in_im, n_near):
    length, groups = step_log.shape
    states = damping.shape[1]
    flat = groups * states
    return pl.pallas_call(
        scan_kernel,
        out_shape=(
            jax.ShapeDtypeStruct((4 * length, flat), F32),
            jax.ShapeDtypeStruct((32, flat), F32),
            jax.ShapeDtypeStruct((n_near, 32, 128), F32),
        ),
        scratch_shapes=[
            pltpu.VMEM((length, 2 * flat), F32),
            pltpu.VMEM((length, flat), F32),
            pltpu.VMEM((length, flat), F32),
            pltpu.VMEM((8, flat), F32),
            pltpu.VMEM((32, 128), F32),
        ],
        compiler_params=pltpu.CompilerParams(vmem_limit_bytes=24 * 2**20),
        cost_estimate=pl.CostEstimate(flops=4 * 10**9, bytes_accessed=3 * 2**20, transcendentals=0),
        name="local_scan",
    )(
        signal, step_log, forget_log, damping, freq,
        in_re.reshape(flat, -1), in_im.reshape(flat, -1),
    )


def quarters(value):
    return value[0:8, :], value[8:16, :], value[16:24, :], value[24:32, :]


def joined(first, second):
    a_re, a_im, b_re, b_im = first
    c_re, c_im, d_re, d_im = second
    return (
        c_re * a_re - c_im * a_im, c_re * a_im + c_im * a_re,
        c_re * b_re - c_im * b_im + d_re, c_re * b_im + c_im * b_re + d_im,
    )


def fold_kernel(near_ref, send_ref, inside_ref):
    me = lax.axis_index("sp_1") * lax.axis_size("sp_2") + lax.axis_index("sp_2")
    one, zero = jnp.ones((8, 128), F32), jnp.zeros((8, 128), F32)
    total = inside = (one, zero, zero, zero)
    for k in range(near_ref.shape[0]):
        total = joined(total, quarters(near_ref[k]))
        passed = jnp.broadcast_to(k < me, (8, 128))
        inside = tuple(jnp.where(passed, new, old) for new, old in zip(total, inside))
    inside_ref[...] = jnp.concatenate(inside, axis=0)
    total = jnp.concatenate(total, axis=0)
    for k in range(send_ref.shape[0]):
        send_ref[k] = total


def fold(near, n_far):
    one = near.shape[1:]
    return pl.pallas_call(
        fold_kernel,
        out_shape=(jax.ShapeDtypeStruct((n_far, *one), F32), jax.ShapeDtypeStruct(one, F32)),
        cost_estimate=pl.CostEstimate(flops=10**6, bytes_accessed=2**18, transcendentals=0),
        name="fold",
    )(near)


def readout_kernel(
    far_ref, inside_ref, all_ref, chunk_ref, sig_ref, outre_ref, outim_ref, skip_ref, wout_ref,
    part_ref,
    st_ref, wide_ref,
):
    length, flat = all_ref.shape[0] // 4, all_ref.shape[1]
    outs, states = outre_ref.shape
    groups = flat // states
    width = outs // groups
    z = lax.axis_index("sp_0")
    one, zero = jnp.ones((8, 128), F32), jnp.zeros((8, 128), F32)
    before = (one, zero, zero, zero)
    for k in range(far_ref.shape[0]):
        passed = jnp.broadcast_to(k < z, (8, 128))
        before = tuple(jnp.where(passed, new, old) for new, old in zip(joined(before, quarters(far_ref[k])), before))
    _, _, t_re, t_im = joined(before, quarters(inside_ref[...]))
    b_re = jnp.concatenate([jnp.broadcast_to(t_re[r : r + 1, :], (8, 128)) for r in range(8)], axis=1)
    b_im = jnp.concatenate([jnp.broadcast_to(t_im[r : r + 1, :], (8, 128)) for r in range(8)], axis=1)
    c_re, c_im = chunk_ref[0:8, :], chunk_ref[8:16, :]
    first_re = c_re * b_re - c_im * b_im + chunk_ref[16:24, :]
    first_im = c_re * b_im + c_im * b_re + chunk_ref[24:32, :]
    for i in range(length // 16):
        pair_re, pair_im = [], []
        for h in range(2):
            l_re, l_im, q_re, q_im = (all_ref[pl.ds(k * length + i * 16 + h * 8, 8), :] for k in range(4))
            pair_re.append(l_re + q_re * first_re - q_im * first_im)
            pair_im.append(l_im + q_re * first_im + q_im * first_re)
        rows = pl.ds(i * 16, 16)
        st_ref[rows, 0:flat] = jnp.concatenate(pair_re, axis=0).astype(BF16)
        st_ref[rows, flat : 2 * flat] = jnp.concatenate(pair_im, axis=0).astype(BF16)
    tile = ones_where(iota((states, flat), 0) == iota((states, flat), 1) % states, BF16)
    mine = iota((outs, flat), 0) // width == iota((outs, flat), 1) // states
    wide_ref[:, 0:flat] = jnp.where(mine, dot(outre_ref[...], tile), 0.0).astype(BF16)
    wide_ref[:, flat : 2 * flat] = jnp.where(mine, -dot(outim_ref[...], tile), 0.0).astype(BF16)
    order = ones_where(token_order(length), BF16)
    sig = dot(order, sig_ref[...])
    value = lax.dot_general(st_ref[...], wide_ref[...], TO_LAST, preferred_element_type=F32) + skip_ref[...] * sig
    cube = 0.7978845608028654 * (value + 0.044715 * (value * value * value))
    mixed = (0.5 * value * (1.0 + jnp.tanh(cube))).astype(BF16)
    back = lax.dot_general(order, mixed, (((0,), (0,)), ((), ())), preferred_element_type=F32).astype(BF16)
    n_part, cols = part_ref.shape[0], part_ref.shape[2]
    for k in range(n_part):
        part_ref[k] = dot(back, wout_ref[:, k * cols : (k + 1) * cols]).astype(BF16)


def readout(far, inside, scanned, chunk, signal, out_re, out_im, skip, w_out, n_tp):
    length, flat = scanned.shape[0] // 4, scanned.shape[1]
    states = out_re.shape[2]
    outs = out_re.shape[0] * out_re.shape[1]
    model = w_out.shape[1]
    return pl.pallas_call(
        readout_kernel,
        out_shape=jax.ShapeDtypeStruct((n_tp, length, model // n_tp), BF16),
        scratch_shapes=[pltpu.VMEM((length, 2 * flat), BF16), pltpu.VMEM((outs, 2 * flat), BF16)],
        compiler_params=pltpu.CompilerParams(vmem_limit_bytes=24 * 2**20),
        cost_estimate=pl.CostEstimate(flops=4 * 10**9, bytes_accessed=4 * 2**20, transcendentals=0),
        name="readout",
    )(
        far, inside, scanned, chunk, signal,
        out_re.reshape(outs, states), out_im.reshape(outs, states), skip.reshape(1, outs), w_out,
    )


def middle_kernel(part_ref, res_ref, gain_ref, mid_ref):
    length = res_ref.shape[0]
    total = res_ref[...].astype(F32)
    added = part_ref[0].astype(F32)
    for k in range(1, part_ref.shape[0]):
        added = added + part_ref[k].astype(F32)
    mid_ref[0:length, :] = (total + added).astype(BF16)
    extra = mid_ref.shape[0] - length
    mid_ref[length:, :] = jnp.broadcast_to(gain_ref[...], (extra, gain_ref.shape[1]))


def middle_of(parts, residual, gain):
    length, cols = residual.shape
    return pl.pallas_call(
        middle_kernel,
        out_shape=jax.ShapeDtypeStruct((length + 16, cols), BF16),
        cost_estimate=pl.CostEstimate(flops=10**6, bytes_accessed=2**20, transcendentals=0),
        name="middle",
    )(parts, residual, gain.reshape(1, cols))


def split_kernel(wg_ref, wu_ref, wd_ref, mine_ref, other_ref, down_ref):
    half = down_ref.shape[2]
    north = lax.axis_index("sp_2") == 1
    for ref, at in ((wg_ref, 0), (wu_ref, half)):
        low, high = ref[:, 0:half], ref[:, half:]
        mine_ref[:, at : at + half] = jnp.where(north, high, low)
        other_ref[:, at : at + half] = jnp.where(north, low, high)
    for c in range(2):
        down = wd_ref[:, c * half : (c + 1) * half]
        for k in range(down_ref.shape[0] // 2):
            down_ref[2 * k + c] = down


def split(w_gate, w_up, w_down, n_x):
    rows, hidden = w_gate.shape
    half = hidden // 2
    return pl.pallas_call(
        split_kernel,
        out_shape=(
            jax.ShapeDtypeStruct((rows, hidden), BF16),
            jax.ShapeDtypeStruct((rows, hidden), BF16),
            jax.ShapeDtypeStruct((n_x * 2, rows, half), BF16),
        ),
        cost_estimate=pl.CostEstimate(flops=10**6, bytes_accessed=2**21, transcendentals=0),
        name="split",
    )(w_gate, w_up, w_down)


def norm_kernel(mid_ref, out_ref):
    n_tp, rows, cols = mid_ref.shape
    length = rows - 16
    squares = jnp.zeros((length, 1), F32)
    for k in range(n_tp):
        m = mid_ref[k, 0:length, :].astype(F32)
        squares = squares + jnp.sum(m * m, axis=1, keepdims=True)
    scale = lax.rsqrt(squares / (n_tp * cols) + EPS)
    for k in range(n_tp):
        m = mid_ref[k, 0:length, :].astype(F32)
        gain = mid_ref[k, length : length + 1, :].astype(F32)
        out_ref[:, k * cols : (k + 1) * cols] = (m * scale * gain).astype(BF16)


def norm(mid):
    n_tp, rows, cols = mid.shape
    return pl.pallas_call(
        norm_kernel,
        out_shape=jax.ShapeDtypeStruct((rows - 16, n_tp * cols), BF16),
        cost_estimate=pl.CostEstimate(flops=10**6, bytes_accessed=2**20, transcendentals=0),
        name="norm",
    )(mid)


def ffn_kernel(own_ref, other_ref, down_hbm, *refs, n_z, n_x):
    sources = refs[: n_x + 1]
    mine_ref, theirs_ref, lhs_ref, rows_ref, down_ref, sem = refs[n_x + 1 :]
    length, model = own_ref.shape
    tall, hidden2 = rows_ref.shape[1:]
    half = hidden2 // 2
    wide = model // n_z
    cols = mine_ref.shape[2]
    part = wide // n_x
    middle = tall // 2
    targets = [
        rows_ref.at[0], rows_ref.at[1], rows_ref.at[2, 0:middle, :], rows_ref.at[2, middle:tall, :], rows_ref.at[3],
    ]
    copies = [pltpu.make_async_copy(src, dst, sem.at[k]) for k, (src, dst) in enumerate(zip(sources, targets))]
    copies.append(pltpu.make_async_copy(down_hbm, down_ref, sem.at[n_x + 1]))
    for copy in copies:
        copy.start()
    x = lax.axis_index("sp_1")
    row, col = iota((wide, wide), 0), iota((wide, wide), 1)
    turned = ones_where(row == (col // part + x) % n_x * part + col % part, BF16)
    for k in range(n_z):
        at = slice(k * wide, (k + 1) * wide)
        lhs_ref[0:length, at] = dot(own_ref[:, at], turned).astype(BF16)
        lhs_ref[length:, at] = dot(other_ref[:, at], turned).astype(BF16)
    for copy in copies[:-1]:
        copy.wait()
    both = jnp.zeros((2 * length, hidden2), F32)
    for k in range(n_z):
        right = jnp.concatenate([rows_ref[j, k * part : (k + 1) * part, :] for j in range(n_x)], axis=0)
        both = both + dot(lhs_ref[:, k * wide : (k + 1) * wide], right)
    gate, up = both[:, 0:half], both[:, half:]
    hidden = (gate / (1.0 + jnp.exp(-gate)) * up).astype(BF16)
    copies[-1].wait()
    for k in range(mine_ref.shape[0]):
        down = lax.dot_general(
            hidden, down_ref[k * cols : (k + 1) * cols, :], TO_LAST, preferred_element_type=F32
        ).astype(BF16)
        mine_ref[k] = down[0:length, :]
        theirs_ref[k] = down[length:, :]


def ffn(own, other, down, rows, n_tp, n_z, n_x):
    length, model = own.shape
    shape = jax.ShapeDtypeStruct((n_tp, length, model // n_tp), BF16)
    whole = pl.BlockSpec(memory_space=pltpu.VMEM)
    far = pl.BlockSpec(memory_space=pl.ANY)
    return pl.pallas_call(
        functools.partial(ffn_kernel, n_z=n_z, n_x=n_x),
        out_shape=(shape, shape),
        in_specs=[whole, whole, far] + [far] * len(rows),
        out_specs=(whole, whole),
        scratch_shapes=[
            pltpu.VMEM((2 * length, model), BF16),
            pltpu.VMEM((n_x, *rows[0].shape), BF16),
            pltpu.VMEM(down.shape, BF16),
            pltpu.SemaphoreType.DMA((n_x + 2,)),
        ],
        compiler_params=pltpu.CompilerParams(vmem_limit_bytes=56 * 2**20),
        cost_estimate=pl.CostEstimate(flops=4 * 10**9, bytes_accessed=9 * 2**20, transcendentals=0),
        name="ffn",
    )(own, other, down, *rows)


def shift(x, axis, by):
    count = lax.axis_size(axis)
    return lax.ppermute(x, axis, [(i, (i - by) % count) for i in range(count)])


def local(
    signal, step_log, forget_log, damping, freq, in_re, in_im, out_re, out_im, skip,
    w_out, residual, norm_gain, w_gate, w_up, w_down,
):
    sizes = tuple(lax.axis_size(a) for a in SP)
    n_tp = lax.axis_size("tp")
    tie = lax.optimization_barrier
    mine, other, spread = split(w_gate, w_up, w_down.T, sizes[1])
    other = shift(other, "sp_2", 1)
    south = lax.axis_index("sp_2") == 0
    pair = jnp.concatenate([jnp.where(south, mine, other), jnp.where(south, other, mine)], axis=0)
    second = lax.all_gather(pair, "sp_0", axis=0, tiled=True)
    spread = lax.all_to_all(spread, ("sp_1", "sp_2"), 0, 0, tiled=True)
    down = lax.all_gather(spread.reshape(-1, spread.shape[2]), "sp_0", axis=0, tiled=True)
    scanned, chunk, send = local_scan(signal, step_log, forget_log, damping, freq, in_re, in_im, sizes[1] * sizes[2])
    near = lax.all_to_all(send, ("sp_1", "sp_2"), 0, 0, tiled=True)
    send, inside = fold(near, sizes[0])
    far_states = lax.all_to_all(send, "sp_0", 0, 0, tiled=True)
    second, far_states = tie((second, far_states))
    right, left = shift(second, "sp_1", 1), shift(second, "sp_1", -1)
    parts = readout(far_states, inside, scanned, chunk, signal, out_re, out_im, skip, w_out, n_tp)
    parts = lax.all_to_all(parts, "tp", 0, 0, tiled=True)
    mid = middle_of(parts, residual, norm_gain)
    everyone = lax.all_gather(mid, "tp")
    right, left, everyone = tie((right, left, everyone))
    half = right.shape[0] // 2
    low, high = shift(right[:half], "sp_1", 1), shift(left[half:], "sp_1", -1)
    normed = norm(everyone)
    partner = shift(normed, "sp_2", 1)
    own_part, other_part = ffn(
        normed, partner, down, [second, right, low, high, left], n_tp, sizes[0], sizes[1]
    )
    other_part = shift(other_part, "sp_2", 1)
    total = (own_part.astype(F32) + other_part.astype(F32)).astype(BF16)
    total = lax.all_to_all(total, "tp", 0, 0, tiled=True)
    own = mid[: residual.shape[0]].astype(F32)
    return (own + 0.5 * jnp.sum(total.astype(F32), axis=0)).astype(BF16)


def solution(mesh):
    torus = Mesh(mesh.devices.reshape(8, 4, 2, mesh.shape["tp"]), ("sp_0", "sp_1", "sp_2", "tp"))
    return jax.shard_map(
        local,
        mesh=torus,
        in_specs=(
            P(SP, "tp"), P(SP, "tp"), P(SP, "tp"),
            P("tp", None), P("tp", None),
            P("tp", None, None), P("tp", None, None), P("tp", None, None), P("tp", None, None),
            P("tp"), P("tp", None), P(SP, "tp"), P("tp"),
            P(SP, "tp"), P(SP, "tp"), P("tp", SP),
        ),
        out_specs=P(SP, "tp"),
        check_vma=False,
    )
```

time: 156 us -> 146 us (0.936)
  local copies, waits for them, and re-layouts: 24.5 us -> 8.24 us
  blocking collectives: 57.1 us -> 67.3 us
  waiting for transfers between devices: 26.7 us -> 19.9 us
  starting transfers between devices: 4.59 us -> 9.32 us
  other arithmetic: 7.28 us -> 3.59 us
  Pallas kernels: 20.1 us -> 21.8 us
    all_gather x1 -> x2, waiting for transfers between devices: 18.2 us -> 0.01 us  [the longest x1 0.01 us: local(): second = lax.all_gather(pair, 'sp_0', axis=0, tiled=True)]
    unnamed x39 -> x44, local copies, waits for them, and re-layouts: 22.1 us -> 5.91 us
    ppermute x0 -> x7, waiting for transfers between devices: none -> 12.3 us  [shift(): return lax.ppermute(x, axis, [(i, (i - by) % count) for i in range(count)])]
    all_to_all x2 -> x4, blocking collectives: 43.8 us -> 53.4 us  [the longest x1 16.3 us: local(): far_states = lax.all_to_all(send, 'sp_0', 0, 0, tiled=True)]
    ppermute x0 -> x7, starting transfers between devices: none -> 4.78 us  [shift(): return lax.ppermute(x, axis, [(i, (i - by) % count) for i in range(count)])]
    broadcast_in_dim x1 -> x0, other arithmetic: 4.69 us -> none  [copy_for_each(): jnp.broadcast_to(x[None], (count, *x.shape))]
    broadcast_in_dim x2 -> x0, local copies, waits for them, and re-layouts: 1.88 us -> none  [copy_for_each(): jnp.broadcast_to(x[None], (count, *x.shape))]
    slice x0 -> x2, local copies, waits for them, and re-layouts: none -> 1.75 us  [local(): low, high = (shift(right[:half], 'sp_1', 1), shift(left[half:], 'sp_1', -1))]
  transfers between devices with their start and end apart: 2 -> 10, of which waited for: 2 -> 6; matrix products, arithmetic and copies ran while one was open for 11% -> 2% of each run, Pallas kernels for 6% -> 8%
where the time goes in v2:
time: 146 us; the launch traced here: 144 us
  blocking collectives  67.3 us (46%)
  Pallas kernels  21.8 us (15%)
  waiting for transfers between devices  19.9 us (14%)
  between operations  13.6 us (9%)
  starting transfers between devices  9.32 us (6%)
  local copies, waits for them, and re-layouts  8.24 us (6%)
  other arithmetic  3.59 us (2%)
    all_to_all x1, blocking collectives, local(): far_states = lax.all_to_all(send, 'sp_0', 0, 0, tiled=True)  16.3 us
    all_to_all x1, blocking collectives, local(): total = lax.all_to_all(total, 'tp', 0, 0, tiled=True)  14.1 us
    all_gather x1, blocking collectives, local(): everyone = lax.all_gather(mid, 'tp')  13.9 us
    all_to_all x1, blocking collectives, local(): spread = lax.all_to_all(spread, ('sp_1', 'sp_2'), 0, 0, tiled=True)  13.8 us
    ppermute x7, waiting for transfers between devices, shift(): return lax.ppermute(x, axis, [(i, (i - by) % count) for i in range(count)])  12.3 us
    all_to_all x1, blocking collectives, local(): near = lax.all_to_all(send, ('sp_1', 'sp_2'), 0, 0, tiled=True)  9.15 us
    pallas_call x1, Pallas kernels, ffn(): pl.pallas_call(functools.partial(ffn_kernel, n_z=n_z, n_x=n_x), out_shape...  7.84 us
    all_to_all x1, waiting for transfers between devices, local(): parts = lax.all_to_all(parts, 'tp', 0, 0, tiled=True)  7.5 us
  transfers between devices with their start and end apart: 10, of which 6 were waited for; matrix products, arithmetic and copies ran while one was open for 2% of the time, Pallas kernels for 8%

profile of v2, /device:TPU:2, one launch (start us, length us, event | category | flops | bytes accessed | tf_op | source)
XLA Modules:
  0.0 143.6 jit_solution(17021947261583821376)
XLA Ops:
  6.6 2.0 %split.1 = (bf16[32,1408]{1,0:T(8,128)(2,1)}, bf16[32,1408]{1,0:T(8,128)(2,1)}, bf16[8,32,704]{2,1,0:T(8,128)(2,1)}) custom-call(bf16[32,1408]{1,0:T(8,128)(2,1)} %wg_ref.1, bf16[32,1408]{1,0:T(8,128)(2,1)} %wu_ref.1, bf16[32,1408]{1,0:T(8,128)(2,1)} %bitcast.15), custom_call_target="tpu_custom_call" | custom-call | flops 1000000 | bytes 2097152 | tf_op jit(solution)/shard_map/split/pallas_call | solution.py:317
  8.6 1.5 %collective-permute-done = bf16[32,1408]{1,0:T(8,128)(2,1)S(1)} collective-permute-done((bf16[32,1408]{1,0:T(8,128)(2,1)}, bf16[32,1408]{1,0:T(8,128)(2,1)S(1)}, u32[]{:S(2)}, u32[]{:S(2)}) %collective-permute-start) | collective-permute-done | bytes 90144 | tf_op jit(solution)/shard_map/ppermute | solution.py:418
  11.8 13.8 %all_to_all.25 = bf16[8,32,704]{2,1,0:T(8,128)(2,1)} all-to-all(bf16[8,32,704]{2,1,0:T(8,128)(2,1)} %get-tuple-element.30), channel_id=1, replica_groups=mesh['sp_0'=8,'sp_1'=4,'sp_2'=2,'tp'=4] {'sp_1','sp_2'}, dimensions={0} | all-to-all | bytes 720896 | tf_op jit(solution)/shard_map/all_to_all | solution.py:433
  26.3 4.2 %local_scan.1 = (f32[512,1024]{1,0:T(8,128)S(1)}, f32[32,1024]{1,0:T(8,128)S(1)}, f32[8,32,128]{2,1,0:T(8,128)S(1)}) custom-call(bf16[128,256]{1,0:T(8,128)(2,1)S(1)} %copy-done.1, f32[128,16]{1,0:T(8,128)S(1)} %copy.19.step_ref, f32[128,16]{1,0:T(8,128)S(1)} %copy.20.forget_ref, f32[16,64]{1,0:T(8,128)S(1)} %copy-done.5, f32[16,64]{1,0:T(8,128)S(1)} %copy-done.6, ...), custom_call_target="tpu_custom_call" | custom-call | flops 4000000000 | bytes 3145728 | tf_op jit(solution)/shard_map/local_scan/pallas_call | solution.py:157
  30.5 1.3 copy-done.8
  31.8 9.1 %all_to_all.26.near_ref = f32[8,32,128]{2,1,0:T(8,128)} all-to-all(f32[8,32,128]{2,1,0:T(8,128)S(1)} %get-tuple-element.22), channel_id=1, replica_groups=mesh['sp_0'=8,'sp_1'=4,'sp_2'=2,'tp'=4] {'sp_1','sp_2'}, dimensions={0} | all-to-all | bytes 262144 | tf_op jit(solution)/shard_map/all_to_all | solution.py:436
  40.9 1.6 %fold.1 = (f32[8,32,128]{2,1,0:T(8,128)}, f32[32,128]{1,0:T(8,128)}) custom-call(f32[8,32,128]{2,1,0:T(8,128)} %all_to_all.26.near_ref), custom_call_target="tpu_custom_call" | custom-call | flops 1000000 | bytes 262144 | tf_op jit(solution)/shard_map/fold/pallas_call | solution.py:209
  42.5 16.3 %all_to_all.27.far_ref = f32[8,32,128]{2,1,0:T(8,128)S(1)} all-to-all(f32[8,32,128]{2,1,0:T(8,128)} %get-tuple-element.23), channel_id=1, replica_groups=mesh['sp_0'=8,'sp_1'=4,'sp_2'=2,'tp'=4] {'sp_0'}, dimensions={0} | all-to-all | bytes 262144 | tf_op jit(solution)/shard_map/all_to_all | solution.py:438
  59.1 1.8 %collective-permute-start.1 = (bf16[512,1408]{1,0:T(8,128)(2,1)}, bf16[512,1408]{1,0:T(8,128)(2,1)}, u32[]{:S(2)}, u32[]{:S(2)}) collective-permute-start(bf16[512,1408]{1,0:T(8,128)(2,1)} %all-gather.4.cloned.1.call-done.refs_0_), channel_id=1, source_target_pairs={{0,24},{8,0},{16,8},{24,16},{1,25},{9,1},{17,9},{25,17},{2,26},{10... | collective-permute-start | bytes 4325384 | tf_op jit(solution)/shard_map/ppermute | solution.py:418
  61.6 1.6 %copy-done.9 = f32[512,1024]{1,0:T(8,128)S(1)} copy-done((f32[512,1024]{1,0:T(8,128)S(1)}, f32[512,1024]{1,0:T(8,128)}, u32[]{:S(2)}) %copy-start.9) | copy-done | bytes 2097176
  63.2 2.1 %readout.1 = bf16[4,128,512]{2,1,0:T(8,128)(2,1)} custom-call(f32[8,32,128]{2,1,0:T(8,128)S(1)} %all_to_all.27.far_ref, f32[32,128]{1,0:T(8,128)S(1)} %copy-done.4, f32[512,1024]{1,0:T(8,128)S(1)} %copy-done.9, f32[32,1024]{1,0:T(8,128)S(1)} %get-tuple-element.27.chunk_ref, bf16[128,256]{1,0:T(8,128)(2,1)S(1)} %copy-done.1, bf16[256,64]{1,0:T(8,128)(2,1)S(1)} %bitcast.10, ...), custom_call_target="tpu_custom_call" | custom-call | flops 4000000000 | bytes 4194304 | tf_op jit(solution)/shard_map/readout/pallas_call | solution.py:267
  65.4 4.5 %all-to-all-start.2 = ((bf16[4,128,512]{2,1,0:T(8,128)(2,1)}), bf16[4,128,512]{2,1,0:T(8,128)(2,1)S(1)}, u32[]{:S(2)}, u32[]{:S(2)}) async-start(bf16[4,128,512]{2,1,0:T(8,128)(2,1)} %readout.1), calls=%async_computation.2 | async-start | bytes 1048576 | tf_op jit(solution)/shard_map/all_to_all | solution.py:442
  70.4 7.5 %all-to-all-done.2.part_ref = bf16[4,128,512]{2,1,0:T(8,128)(2,1)S(1)} async-done(((bf16[4,128,512]{2,1,0:T(8,128)(2,1)}), bf16[4,128,512]{2,1,0:T(8,128)(2,1)S(1)}, u32[]{:S(2)}, u32[]{:S(2)}) %all-to-all-start.2) | async-done | bytes 524320 | tf_op jit(solution)/shard_map/all_to_all | solution.py:442
  78.7 1.9 %middle.1 = bf16[144,512]{1,0:T(8,128)(2,1)} custom-call(bf16[4,128,512]{2,1,0:T(8,128)(2,1)} %copy-done.10, bf16[128,512]{1,0:T(8,128)(2,1)} %res_ref.1, bf16[1,512]{1,0:T(2,128)(2,1)} %reshape.26.gain_ref), custom_call_target="tpu_custom_call" | custom-call | flops 1000000 | bytes 1048576 | tf_op jit(solution)/shard_map/middle/pallas_call | solution.py:293
  80.6 13.9 %all-gather = bf16[576,512]{1,0:T(8,128)(2,1)} all-gather(bf16[144,512]{1,0:T(8,128)(2,1)} %middle.1), channel_id=2, replica_groups=mesh['sp_0'=8,'sp_1'=4,'sp_2'=2,'tp'=4] {'tp'}, dimensions={0}, use_global_device_ids=true | all-gather | bytes 737280 | tf_op jit(solution)/shard_map/all_gather | solution.py:444
  94.5 1.7 %slice.10 = bf16[256,1408]{1,0:T(8,128)(2,1)S(1)} slice(bf16[512,1408]{1,0:T(8,128)(2,1)} %collective-permute-done.1.refs_1_), slice={[0:256], [0:1408]} | slice | bytes 1441792 | tf_op jit(solution)/shard_map/slice | solution.py:447
  96.5 2.4 %collective-permute-start.4 = (bf16[256,1408]{1,0:T(8,128)(2,1)S(1)}, bf16[256,1408]{1,0:T(8,128)(2,1)S(1)}, u32[]{:S(2)}, u32[]{:S(2)}) collective-permute-start(bf16[256,1408]{1,0:T(8,128)(2,1)S(1)} %slice.10), channel_id=1, source_target_pairs={{0,24},{8,0},{16,8},{24,16},{1,25},{9,1},{17,9},{25,17},{2,26},{10... | collective-permute-start | bytes 2162696 | tf_op jit(solution)/shard_map/ppermute | solution.py:418
  98.9 2.1 %norm.1.own_ref = bf16[128,2048]{1,0:T(8,128)(2,1)} custom-call(bf16[4,144,512]{2,1,0:T(8,128)(2,1)} %bitcast.13), custom_call_target="tpu_custom_call" | custom-call | flops 1000000 | bytes 1048576 | tf_op jit(solution)/shard_map/norm/pallas_call | solution.py:345
  101.0 2.1 %collective-permute-done.3.other_ref = bf16[128,2048]{1,0:T(8,128)(2,1)S(1)} collective-permute-done((bf16[128,2048]{1,0:T(8,128)(2,1)}, bf16[128,2048]{1,0:T(8,128)(2,1)S(1)}, u32[]{:S(2)}, u32[]{:S(2)}) %collective-permute-start.3) | collective-permute-done | bytes 524320 | tf_op jit(solution)/shard_map/ppermute | solution.py:418
  103.1 6.2 %collective-permute-done.5.refs_3_ = bf16[256,1408]{1,0:T(8,128)(2,1)} collective-permute-done((bf16[256,1408]{1,0:T(8,128)(2,1)S(1)}, bf16[256,1408]{1,0:T(8,128)(2,1)}, u32[]{:S(2)}, u32[]{:S(2)}) %collective-permute-start.5) | collective-permute-done | bytes 720928 | tf_op jit(solution)/shard_map/ppermute | solution.py:418
  110.6 7.8 %ffn.1 = (bf16[4,128,512]{2,1,0:T(8,128)(2,1)}, bf16[4,128,512]{2,1,0:T(8,128)(2,1)}) custom-call(bf16[128,2048]{1,0:T(8,128)(2,1)} %norm.1.own_ref, bf16[128,2048]{1,0:T(8,128)(2,1)} %copy-done.19, bf16[2048,704]{1,0:T(8,128)(2,1)} %all-gather.6.cloned.1.call-done.down_hbm, bf16[512,1408]{1,0:T(8,128)(2,1)} %all-gather.4.cloned.1.call-done.refs_0_, ...), custom_call_target="tpu_custom_call" | custom-call | flops 4000000000 | bytes 9437184 | tf_op jit(solution)/shard_map/ffn/pallas_call | solution.py:399
  118.6 2.1 %collective-permute-done.6 = bf16[4,128,512]{2,1,0:T(8,128)(2,1)S(1)} collective-permute-done((bf16[4,128,512]{2,1,0:T(8,128)(2,1)}, bf16[4,128,512]{2,1,0:T(8,128)(2,1)S(1)}, u32[]{:S(2)}, u32[]{:S(2)}) %collective-permute-start.6) | collective-permute-done | bytes 524320 | tf_op jit(solution)/shard_map/ppermute | solution.py:418
  120.7 1.2 add_convert_fusion
  121.9 14.1 %all_to_all.28 = bf16[4,128,512]{2,1,0:T(8,128)(2,1)S(1)} all-to-all(bf16[4,128,512]{2,1,0:T(8,128)(2,1)S(1)} %add_convert_fusion), channel_id=1, replica_groups=mesh['sp_0'=8,'sp_1'=4,'sp_2'=2,'tp'=4] {'tp'}, dimensions={0} | all-to-all | bytes 1048576 | tf_op jit(solution)/shard_map/all_to_all | solution.py:455
  (62 shorter events, 7.1 us)
Async XLA Ops:
  6.5 19.1 %copy-start.15 = (f32[128,16]{0,1:T(8,128)S(1)}, f32[128,16]{0,1:T(8,128)}, u32[]{:S(2)}) copy-start(f32[128,16]{0,1:T(8,128)} %param.17) | copy-start | bytes 24580
  6.5 19.2 %copy-start.16 = (f32[128,16]{0,1:T(8,128)S(1)}, f32[128,16]{0,1:T(8,128)}, u32[]{:S(2)}) copy-start(f32[128,16]{0,1:T(8,128)} %param.18) | copy-start | bytes 24580
  6.5 19.3 %copy-start.13 = (bf16[16,64,16]{1,2,0:T(8,128)(2,1)S(1)}, bf16[16,64,16]{1,2,0:T(8,128)(2,1)}, u32[]{:S(2)}) copy-start(bf16[16,64,16]{1,2,0:T(8,128)(2,1)} %param.21) | copy-start | bytes 98308
  6.5 19.5 %copy-start.14 = (bf16[16,64,16]{1,2,0:T(8,128)(2,1)S(1)}, bf16[16,64,16]{1,2,0:T(8,128)(2,1)}, u32[]{:S(2)}) copy-start(bf16[16,64,16]{1,2,0:T(8,128)(2,1)} %param.22) | copy-start | bytes 98308
  6.5 52.3 %all-gather.4.cloned.1.call-start = ((), (), s32[]{:S(2)}) async-start(), calls=%async_computation.5 | async-start | bytes 1622016 | tf_op jit(solution)/shard_map/all_gather | solution.py:432
  8.6 1.5 %collective-permute-start = (bf16[32,1408]{1,0:T(8,128)(2,1)}, bf16[32,1408]{1,0:T(8,128)(2,1)S(1)}, u32[]{:S(2)}, u32[]{:S(2)}) collective-permute-start(bf16[32,1408]{1,0:T(8,128)(2,1)} %get-tuple-element.21), channel_id=1, source_target_pairs={{0,4},{4,0},{1,5},{5,1},{2,6},{6,2},{3,7},{7,3},{8,12},{12,8},{9,1... | collective-permute-start | bytes 270344 | tf_op jit(solution)/shard_map/ppermute | solution.py:418
  10.1 16.1 %copy-start.1 = (bf16[128,256]{1,0:T(8,128)(2,1)S(1)}, bf16[128,256]{1,0:T(8,128)(2,1)}, u32[]{:S(2)}) copy-start(bf16[128,256]{1,0:T(8,128)(2,1)} %sig_ref.3) | copy-start | bytes 196612
  10.1 16.1 %copy-start.5 = (f32[16,64]{1,0:T(8,128)S(1)}, f32[16,64]{1,0:T(8,128)}, u32[]{:S(2)}) copy-start(f32[16,64]{1,0:T(8,128)} %damp_ref.1) | copy-start | bytes 12292
  10.1 16.1 %copy-start.6 = (f32[16,64]{1,0:T(8,128)S(1)}, f32[16,64]{1,0:T(8,128)}, u32[]{:S(2)}) copy-start(f32[16,64]{1,0:T(8,128)} %freq_ref.1) | copy-start | bytes 12292
  11.7 98.0 %all-gather.6.cloned.1.call-start = ((), (), s32[]{:S(2)}) async-start(), calls=%async_computation.6 | async-start | bytes 3538944 | tf_op jit(solution)/shard_map/all_gather | solution.py:434
  26.2 34.7 %copy-start = (bf16[256,2048]{1,0:T(8,128)(2,1)S(1)}, bf16[256,2048]{1,0:T(8,128)(2,1)}, u32[]{:S(2)}) copy-start(bf16[256,2048]{1,0:T(8,128)(2,1)} %wout_ref.1) | copy-start | bytes 3145732
  26.2 34.7 %copy-start.2 = (bf16[16,16,64]{2,1,0:T(8,128)(2,1)S(1)}, bf16[16,16,64]{2,1,0:T(8,128)(2,1)}, u32[]{:S(2)}) copy-start(bf16[16,16,64]{2,1,0:T(8,128)(2,1)} %param.23) | copy-start | bytes 98308
  26.3 34.7 %copy-start.3 = (bf16[16,16,64]{2,1,0:T(8,128)(2,1)S(1)}, bf16[16,16,64]{2,1,0:T(8,128)(2,1)}, u32[]{:S(2)}) copy-start(bf16[16,16,64]{2,1,0:T(8,128)(2,1)} %param.24) | copy-start | bytes 98308
  26.3 34.6 %copy-start.7 = (f32[256]{0:T(256)S(1)}, f32[256]{0:T(256)}, u32[]{:S(2)}) copy-start(f32[256]{0:T(256)} %param.25) | copy-start | bytes 3076
  58.9 35.6 %collective-permute-start.2 = (bf16[512,1408]{1,0:T(8,128)(2,1)}, bf16[512,1408]{1,0:T(8,128)(2,1)S(1)}, u32[]{:S(2)}, u32[]{:S(2)}) collective-permute-start(bf16[512,1408]{1,0:T(8,128)(2,1)} %all-gather.4.cloned.1.call-done.refs_0_), channel_id=1, source_target_pairs={{0,8},{8,16},{16,24},{24,0},{1,9},{9,17},{17,25},{25,1},{2,10},{10... | collective-permute-start | bytes 4325384 | tf_op jit(solution)/shard_map/ppermute | solution.py:418
  59.1 35.3 %collective-permute-start.1 = (bf16[512,1408]{1,0:T(8,128)(2,1)}, bf16[512,1408]{1,0:T(8,128)(2,1)}, u32[]{:S(2)}, u32[]{:S(2)}) collective-permute-start(bf16[512,1408]{1,0:T(8,128)(2,1)} %all-gather.4.cloned.1.call-done.refs_0_), channel_id=1, source_target_pairs={{0,24},{8,0},{16,8},{24,16},{1,25},{9,1},{17,9},{25,17},{2,26},{10... | collective-permute-start | bytes 4325384 | tf_op jit(solution)/shard_map/ppermute | solution.py:418
  63.2 6.6 %copy-start.17 = (bf16[512]{0:T(512)(128)(2,1)S(1)}, bf16[512]{0:T(512)(128)(2,1)}, u32[]{:S(2)}) copy-start(bf16[512]{0:T(512)(128)(2,1)} %param.28) | copy-start | bytes 3076
  65.4 12.5 %all-to-all-start.2 = ((bf16[4,128,512]{2,1,0:T(8,128)(2,1)}), bf16[4,128,512]{2,1,0:T(8,128)(2,1)S(1)}, u32[]{:S(2)}, u32[]{:S(2)}) async-start(bf16[4,128,512]{2,1,0:T(8,128)(2,1)} %readout.1), calls=%async_computation.2 | async-start | bytes 1048576 | tf_op jit(solution)/shard_map/all_to_all | solution.py:442
  96.2 13.1 %collective-permute-start.5 = (bf16[256,1408]{1,0:T(8,128)(2,1)S(1)}, bf16[256,1408]{1,0:T(8,128)(2,1)}, u32[]{:S(2)}, u32[]{:S(2)}) collective-permute-start(bf16[256,1408]{1,0:T(8,128)(2,1)S(1)} %slice.11), channel_id=1, source_target_pairs={{0,8},{8,16},{16,24},{24,0},{1,9},{9,17},{17,25},{25,1},{2,10},{10... | collective-permute-start | bytes 2162696 | tf_op jit(solution)/shard_map/ppermute | solution.py:418
  96.5 13.3 %collective-permute-start.4 = (bf16[256,1408]{1,0:T(8,128)(2,1)S(1)}, bf16[256,1408]{1,0:T(8,128)(2,1)S(1)}, u32[]{:S(2)}, u32[]{:S(2)}) collective-permute-start(bf16[256,1408]{1,0:T(8,128)(2,1)S(1)} %slice.10), channel_id=1, source_target_pairs={{0,24},{8,0},{16,8},{24,16},{1,25},{9,1},{17,9},{25,17},{2,26},{10... | collective-permute-start | bytes 2162696 | tf_op jit(solution)/shard_map/ppermute | solution.py:418
  101.0 2.1 %collective-permute-start.3 = (bf16[128,2048]{1,0:T(8,128)(2,1)}, bf16[128,2048]{1,0:T(8,128)(2,1)S(1)}, u32[]{:S(2)}, u32[]{:S(2)}) collective-permute-start(bf16[128,2048]{1,0:T(8,128)(2,1)} %norm.1.own_ref), channel_id=1, source_target_pairs={{0,4},{4,0},{1,5},{5,1},{2,6},{6,2},{3,7},{7,3},{8,12},{12,8},{9,1... | collective-permute-start | bytes 1572872 | tf_op jit(solution)/shard_map/ppermute | solution.py:418
  103.1 6.6 %copy-start.19 = (bf16[128,2048]{1,0:T(8,128)(2,1)}, bf16[128,2048]{1,0:T(8,128)(2,1)S(1)}, u32[]{:S(2)}) copy-start(bf16[128,2048]{1,0:T(8,128)(2,1)S(1)} %collective-permute-done.3.other_ref) | copy-start | bytes 1572868
  118.5 2.2 %collective-permute-start.6 = (bf16[4,128,512]{2,1,0:T(8,128)(2,1)}, bf16[4,128,512]{2,1,0:T(8,128)(2,1)S(1)}, u32[]{:S(2)}, u32[]{:S(2)}) collective-permute-start(bf16[4,128,512]{2,1,0:T(8,128)(2,1)} %get-tuple-element.34), channel_id=1, source_target_pairs={{0,4},{4,0},{1,5},{5,1},{2,6},{6,2},{3,7},{7,3},{8,12},{12,8},{9,1... | collective-permute-start | bytes 1572872 | tf_op jit(solution)/shard_map/ppermute | solution.py:418
  120.7 15.4 %copy-start.11 = (bf16[144,512]{1,0:T(8,128)(2,1)S(1)}, bf16[144,512]{1,0:T(8,128)(2,1)}, u32[]{:S(2)}) copy-start(bf16[144,512]{1,0:T(8,128)(2,1)} %middle.1) | copy-start | bytes 442372
  (6 other events, 7.1 us)
Sparse Core Ops, SparseCore 0:
  11.9 42.5 all-gather.3
  56.2 44.1 all-gather.5
